TPU v7x, 32 devices: a whole 2x2x4 slice. The times are simulated.
32 devices in a mesh: dp: 4 (over y, x), kv: 4 (over z), tp: 2 (over core).
Axes of the slice: x: 2, y: 2, z: 4, core: 2. Of those that a mesh axis runs over, the one named last changes fastest.
Arguments:
- tokens: bfloat16 [4096, 4096], P(('dp', 'kv')), parts along dimension 0, may hold values from -16 to 16
- query_weight: bfloat16 [4096, 1024], P('kv', 'tp'), may hold values from -0.09375 to 0.09375
- key_weight: bfloat16 [4096, 256], P('kv', 'tp'), may hold values from -0.09375 to 0.09375
- value_weight: bfloat16 [4096, 256], P('kv', 'tp'), may hold values from -0.09375 to 0.09375
- out_weight: bfloat16 [1024, 4096], P('kv', 'tp'), may hold values from -1.5 to 1.5
- chosen: int32 [128, 16], P(('dp', 'kv')), parts along dimension 0, may hold values from -1 to 31, as said below
- live_length: int32 [4], P('dp'), parts along dimension 0, may hold values from 128 to 1024
Outputs:
- mixed: bfloat16 [4096, 4096], P(('dp', 'kv'), 'tp'), parts along dimension 0
There are 4 independent parts, one for each index of `dp`. A program takes and returns all parts, laid end to end along the dimension named above; an argument that names none is the same for every part. Nothing has to cross between parts.
Inputs may be any that keep to these rules, and one draw needn't show every extreme that they name: `chosen`: row j lists 16 entries: entry 0 is j itself, the others are distinct blocks before j, or -1 for unused entries. The query blocks of one device together read at most 2 distinct blocks held by any one other device, and some device reads 2 of another's in every draw.
All inputs are finite; a program needn't handle non-finite values.
Results may differ from a plain program's by a relative error of at most 0.0085.
Values may be sent and summed in bfloat16 or wider, within the bound.
A program may use at most 64 MiB of HBM per device.

v0:
```python
import functools

import jax
import jax.numpy as jnp
from jax import lax
from jax.experimental import pallas as pl
from jax.experimental.pallas import tpu as pltpu
from jax.sharding import PartitionSpec as P

HD = 128
BLOCK = 32
CAP = 2
MESH = pl.DeviceIdType.MESH


def gathered_body(tokens, query_weight, key_weight, value_weight, out_weight, chosen, live_length):
    rows = tokens.shape[0]
    per_dev = rows // BLOCK
    owners = lax.axis_size("kv")
    me = lax.axis_index("kv")

    def add_rows(piece):
        return jnp.dot(tokens, piece, preferred_element_type=jnp.float32)

    queries = add_rows(lax.all_gather(query_weight, "kv", axis=0, tiled=True))
    keys = add_rows(lax.all_gather(key_weight, "kv", axis=0, tiled=True))
    values = add_rows(lax.all_gather(value_weight, "kv", axis=0, tiled=True))
    queries = queries.astype(jnp.bfloat16)
    paired = jnp.concatenate([keys.astype(jnp.bfloat16), values.astype(jnp.bfloat16)], axis=1)
    width = paired.shape[1]
    local_blocks = paired.reshape(per_dev, BLOCK, width)
    valid = chosen >= 0
    safe = jnp.maximum(chosen, 0)
    blocks_all = owners * per_dev
    hits = (safe[:, :, None] == jnp.arange(blocks_all, dtype=jnp.int32)[None, None, :]) & valid[
        :, :, None
    ]
    needed = jnp.any(hits, axis=(0, 1)).reshape(owners, per_dev)
    needed = needed & (jnp.arange(owners, dtype=jnp.int32) != me)[:, None]
    ranks = jnp.cumsum(needed.astype(jnp.int32), axis=1)
    local_ids = jnp.arange(per_dev, dtype=jnp.int32)
    slot_lists = []
    for slot in range(CAP):
        marked = needed & (ranks == slot + 1)
        found = jnp.any(marked, axis=1)
        where_at = jnp.sum(jnp.where(marked, local_ids[None, :], 0), axis=1)
        slot_lists.append(jnp.where(found, where_at, -1))
    wanted = jnp.stack(slot_lists, axis=1)
    requested = lax.all_to_all(wanted, "kv", split_axis=0, concat_axis=0, tiled=True)
    outgoing = local_blocks[jnp.maximum(requested, 0)]
    outgoing = jnp.where((requested >= 0)[:, :, None, None], outgoing, jnp.zeros((), jnp.bfloat16))
    incoming = lax.all_to_all(outgoing, "kv", split_axis=0, concat_axis=0, tiled=True)
    table = jnp.concatenate([incoming.reshape(owners * CAP, BLOCK, width), local_blocks], axis=0)
    segment_retainer = safe // per_dev
    local_of = safe % per_dev
    match = (wanted[None, None, :, :] == local_of[:, :, None, None]) & (
        jnp.arange(owners, dtype=jnp.int32)[None, None, :, None]
        == segment_retainer[:, :, None, None]
    )
    slot_index = jnp.arange(owners * CAP, dtype=jnp.int32).reshape(owners, CAP)
    remote_at = jnp.sum(jnp.where(match, slot_index[None, None], 0), axis=(2, 3))
    position = jnp.where(segment_retainer == me, owners * CAP + local_of, remote_at)
    picked = table[position]
    near_keys = picked[..., :HD]
    near_values = picked[..., HD:]
    grouped = queries.reshape(per_dev, BLOCK, -1, HD)
    scores = jnp.einsum(
        "jqhd,jnbd->jhqnb", grouped, near_keys, preferred_element_type=jnp.float32
    ) * HD ** (-0.5)
    query_pos = (me * per_dev + jnp.arange(per_dev, dtype=jnp.int32))[:, None] * BLOCK + jnp.arange(
        BLOCK, dtype=jnp.int32
    )[None, :]
    key_pos = safe[:, :, None] * BLOCK + jnp.arange(BLOCK, dtype=jnp.int32)[None, None, :]
    allowed = valid[:, None, :, None] & (key_pos[:, None, :, :] <= query_pos[:, :, None, None])
    masked = jnp.where(allowed[:, None], scores, -jnp.inf)
    top = jnp.max(masked, axis=(3, 4), keepdims=True)
    weights = jnp.exp(masked - top)
    total = jnp.sum(weights, axis=(3, 4))
    summed = jnp.einsum(
        "jhqnb,jnbd->jqhd",
        weights.astype(jnp.bfloat16),
        near_values,
        preferred_element_type=jnp.float32,
    )
    result = summed / jnp.transpose(total, (0, 2, 1))[..., None]
    live = query_pos < live_length[0]
    result = jnp.where(live[:, :, None, None], result, 0.0)
    attended = result.astype(jnp.bfloat16).reshape(rows, -1)
    every_head = lax.all_gather(attended, "tp", axis=1, tiled=True)
    mixed = jnp.dot(
        every_head,
        lax.all_gather(out_weight, "kv", axis=0, tiled=True),
        preferred_element_type=jnp.float32,
    )
    return mixed.astype(jnp.bfloat16)


class Stream:
    def __init__(self, place, full, first, rows, halved, sends, recvs, base):
        self.place, self.full, self.halved = place, full, halved
        self.shard = full.shape[0] // place["n"]
        self.first, self.rows = first, rows
        self.sends, self.recvs, self.base = sends, recvs, base
        self.begun = []

    def part(self, owner, index, count):
        size = self.rows // count
        start = pl.multiple_of(owner * self.shard + self.first + index * size, size)
        return self.full.at[pl.ds(start, size), :]

    def carried(self, owner):
        if self.halved:
            return self.part(owner, self.place["half"], 2)
        return self.part(owner, self.place["dp"], 4)

    def copy(self, part, owner, kind, target, sent_as=None):
        at = self.base + owner * 5
        return pltpu.make_async_remote_copy(
            src_ref=part,
            dst_ref=part,
            send_sem=self.sends.at[at + (kind if sent_as is None else sent_as)],
            recv_sem=self.recvs.at[at + kind],
            device_id=target,
            device_id_type=MESH,
        )

    def begin(self, c, when=None):
        if when is None:
            c.start()
        else:
            pl.when(when)(c.start)
        self.begun.append((c, when))

    def issue(self):
        p = self.place
        me, n = p["me"], p["n"]
        mine = self.carried(me)
        self.begin(self.copy(mine, me, 0, {"kv": p["right"]}), me < n - 1)
        self.begin(self.copy(mine, me, 0, {"kv": p["left"]}, 1), me > 0)

    def relay(self, slot):
        p = self.place
        me, n, owner = p["me"], p["n"], p["order"][slot]
        piece = self.carried(owner)
        self.copy(piece, owner, 0, {"kv": p["right"]}).wait_recv()
        self.begin(
            self.copy(piece, owner, 0, {"kv": p["right"]}), jnp.logical_and(owner < me, me < n - 1)
        )
        self.begin(self.copy(piece, owner, 0, {"kv": p["left"]}, 0), jnp.logical_and(owner > me, me > 0))
        if self.halved:
            to_x = self.part(owner, 2 * p["half"], 4)
            to_y = self.part(owner, 2 * p["half"] + 1, 4)
        else:
            to_x = to_y = piece
        self.begin(self.copy(to_x, owner, 1, {"dp": p["x"]}))
        self.begin(self.copy(to_y, owner, 2, {"dp": p["y"]}))

    def corner(self, slot):
        p = self.place
        owner = p["order"][slot]
        if self.halved:
            other = 2 * (1 - p["half"])
            self.copy(self.part(owner, other, 4), owner, 1, {"dp": p["x"]}).wait_recv()
            self.copy(self.part(owner, other + 1, 4), owner, 2, {"dp": p["y"]}).wait_recv()
            return
        self.copy(self.part(owner, p["x"], 4), owner, 1, {"dp": p["x"]}).wait_recv()
        self.begin(self.copy(self.part(owner, 2 * p["x"], 8), owner, 4, {"dp": p["y"]}))
        self.copy(self.part(owner, p["y"], 4), owner, 2, {"dp": p["y"]}).wait_recv()
        self.begin(self.copy(self.part(owner, 2 * p["y"] + 1, 8), owner, 3, {"dp": p["x"]}))

    def arrive(self):
        p = self.place
        if self.halved:
            return
        for owner in p["order"]:
            self.copy(self.part(owner, 2 * p["far"], 8), owner, 4, {"dp": p["y"]}).wait_recv()
            self.copy(self.part(owner, 2 * p["far"] + 1, 8), owner, 3, {"dp": p["x"]}).wait_recv()

    def finish(self):
        for c, when in self.begun:
            if when is None:
                c.wait_send()
            else:
                pl.when(when)(c.wait_send)


def kernel(
    n, chosen, live, tokens, query_w, key_w, value_w, out_w, mixed,
    tok, full_q, full_k, full_v, full_o, paired, queries, bias, attended,
    local_sem, send_sem, recv_sem, kv_send, kv_recv, tp_send, tp_recv,
):
    dp, me, tp = lax.axis_index("dp"), lax.axis_index("kv"), lax.axis_index("tp")
    x_at, y_at = lax.rem(dp, 2), lax.div(dp, 2)
    place = {
        "n": n,
        "me": me,
        "left": lax.rem(me + n - 1, n),
        "right": lax.rem(me + 1, n),
        "opp": lax.rem(me + 2, n),
        "x": 2 * y_at + (1 - x_at),
        "y": 2 * (1 - y_at) + x_at,
        "half": lax.rem(x_at + y_at, 2),
        "dp": dp,
        "far": 2 * (1 - y_at) + (1 - x_at),
    }
    order = []
    for i in range(n - 1):
        up = i + (i >= me).astype(jnp.int32)
        down = n - 1 - i - (n - 1 - i <= me).astype(jnp.int32)
        order.append(jnp.where(2 * me < n, up, down))
    place["order"] = order
    rows = tok.shape[0]
    per_dev = rows // BLOCK
    seq = n * rows

    fulls = (full_k, full_v, full_q, full_o)
    loads = []
    for index, (shard, full) in enumerate(zip((key_w, value_w, query_w, out_w), fulls)):
        size = shard.shape[0]
        mine = full.at[pl.ds(pl.multiple_of(me * size, size), size), :]
        loads.append(pltpu.make_async_copy(shard, mine, local_sem.at[index]))
    loads.append(pltpu.make_async_copy(tokens, tok, local_sem.at[4]))
    for load in loads:
        load.start()

    barrier = pltpu.get_barrier_semaphore()
    greeted = [{"kv": place[k]} for k in ("left", "right", "opp")]
    greeted += [{"dp": place[k]} for k in ("x", "y")] + [{"tp": 1 - tp}]
    for target in greeted:
        pl.semaphore_signal(barrier, inc=1, device_id=target, device_id_type=MESH)
    pl.semaphore_wait(barrier, len(greeted))

    cut = full_o.shape[0] // n // 2
    plan = [(full_k, 0, 0), (full_v, 0, 0), (full_q, 0, 0), (full_o, 0, 0), (full_o, cut, 1)]
    streams = []
    for i, (full, first, halved) in enumerate(plan):
        count = cut if full is full_o else full.shape[0] // n
        streams.append(
            Stream(place, full, first, count, halved, send_sem, recv_sem, 5 * n * i)
        )
    groups = [streams[:2], streams[2:3], streams[3:4], streams[4:5]]
    each = n - 1

    def advance(at):
        group, slot = divmod(at, each)
        if group < len(groups):
            for s in groups[group]:
                s.relay(slot)
            if slot == 0 and group + 1 < len(groups):
                for s in groups[group + 1]:
                    s.issue()
        if at > 0:
            group, slot = divmod(at - 1, each)
            for s in groups[group]:
                s.corner(slot)

    loads[0].wait()
    loads[1].wait()
    for s in groups[0]:
        s.issue()
    loads[2].wait()
    loads[3].wait()
    loads[4].wait()

    column = lax.broadcasted_iota(jnp.int32, (BLOCK, seq), 1)
    row = lax.broadcasted_iota(jnp.int32, (BLOCK, seq), 0)
    key_block = lax.div(lax.broadcasted_iota(jnp.int32, (8, seq), 1), BLOCK)
    for j in range(per_dev):
        listed = jnp.full((8, seq), -jnp.inf, jnp.float32)
        for e in range(chosen.shape[1]):
            listed = jnp.where(key_block == chosen[j, e], 0.0, listed)
        spread = jnp.concatenate([listed] * (BLOCK // 8), axis=0)
        causal = column <= row + (me * rows + j * BLOCK)
        bias[j * BLOCK : (j + 1) * BLOCK, :] = jnp.where(causal, spread, -jnp.inf)

    for at in range(each + 2):
        advance(at)
    for s in groups[0]:
        s.arrive()
    mine = pl.ds(pl.multiple_of(me * rows, rows), rows)
    paired[mine, :HD] = jnp.dot(
        tok[...], full_k[...], preferred_element_type=jnp.float32
    ).astype(jnp.bfloat16)
    paired[mine, HD:] = jnp.dot(
        tok[...], full_v[...], preferred_element_type=jnp.float32
    ).astype(jnp.bfloat16)
    advance(each + 2)
    kv_copies = []
    for step in range(1, n):
        block = paired.at[mine, :]
        c = pltpu.make_async_remote_copy(
            src_ref=block, dst_ref=block,
            send_sem=kv_send.at[step - 1], recv_sem=kv_recv.at[step - 1],
            device_id={"kv": lax.rem(me + step, n)}, device_id_type=MESH,
        )
        c.start()
        kv_copies.append(c)
    for at in range(each + 3, 2 * each + 2):
        advance(at)
    groups[1][0].arrive()
    queries[...] = jnp.dot(
        tok[...], full_q[...], preferred_element_type=jnp.float32
    ).astype(jnp.bfloat16)
    advance(2 * each + 2)
    for step in range(1, n):
        owner = lax.rem(me + n - step, n)
        block = paired.at[pl.ds(pl.multiple_of(owner * rows, rows), rows), :]
        pltpu.make_async_remote_copy(
            src_ref=block, dst_ref=block,
            send_sem=kv_send.at[step - 1], recv_sem=kv_recv.at[step - 1],
            device_id={"kv": lax.rem(me + step, n)}, device_id_type=MESH,
        ).wait_recv()

    position = me * rows + lax.broadcasted_iota(jnp.int32, (rows, HD), 0)
    alive = position < live[0]
    heads = queries.shape[1] // HD
    for h in range(heads):
        cols = slice(h * HD, (h + 1) * HD)
        scores = lax.dot_general(
            queries[:, cols], paired[:, :HD], (((1,), (1,)), ((), ())),
            preferred_element_type=jnp.float32,
        )
        masked = scores * HD ** (-0.5) + bias[...]
        top = jnp.max(masked, axis=1, keepdims=True)
        weights = jnp.exp(masked - top)
        total = jnp.sum(weights, axis=1, keepdims=True)
        summed = jnp.dot(
            weights.astype(jnp.bfloat16), paired[:, HD:], preferred_element_type=jnp.float32
        )
        result = jnp.where(alive, summed / total, 0.0).astype(jnp.bfloat16)
        attended[tp, :, cols] = result
        if h == heads // 2 - 1:
            advance(2 * each + 3)
    share = pltpu.make_async_remote_copy(
        src_ref=attended.at[tp], dst_ref=attended.at[tp],
        send_sem=tp_send, recv_sem=tp_recv, device_id={"tp": 1 - tp}, device_id_type=MESH,
    )
    share.start()
    for at in range(2 * each + 4, len(groups) * each + 1):
        advance(at)
    pltpu.make_async_remote_copy(
        src_ref=attended.at[1 - tp], dst_ref=attended.at[1 - tp],
        send_sem=tp_send, recv_sem=tp_recv, device_id={"tp": 1 - tp}, device_id_type=MESH,
    ).wait_recv()
    for s in groups[2] + groups[3]:
        s.arrive()
    wide = queries.shape[1]
    tile = 512
    for c in range(0, mixed.shape[1], tile):
        acc = jnp.dot(
            attended[0], full_o[:wide, c : c + tile], preferred_element_type=jnp.float32
        )
        acc += jnp.dot(
            attended[1], full_o[wide:, c : c + tile], preferred_element_type=jnp.float32
        )
        mixed[:, c : c + tile] = acc.astype(jnp.bfloat16)
    for s in streams:
        s.finish()
    for c in kv_copies:
        c.wait_send()
    share.wait_send()


def woven_body(tokens, query_weight, key_weight, value_weight, out_weight, chosen, live_length):
    n = lax.axis_size("kv")
    rows, width = tokens.shape
    wide = query_weight.shape[1]
    dma = pltpu.SemaphoreType.DMA
    bf16 = jnp.bfloat16
    anywhere = pl.BlockSpec(memory_space=pl.ANY)
    small = pl.BlockSpec(memory_space=pltpu.SMEM)
    return pl.pallas_call(
        functools.partial(kernel, n),
        out_shape=jax.ShapeDtypeStruct((rows, out_weight.shape[1]), bf16),
        in_specs=[small, small] + [anywhere] * 5,
        out_specs=pl.BlockSpec(memory_space=pltpu.VMEM),
        scratch_shapes=[
            pltpu.VMEM((rows, width), bf16),
            pltpu.VMEM((width, wide), bf16),
            pltpu.VMEM((width, HD), bf16),
            pltpu.VMEM((width, HD), bf16),
            pltpu.VMEM((n * out_weight.shape[0], out_weight.shape[1]), bf16),
            pltpu.VMEM((n * rows, 2 * HD), bf16),
            pltpu.VMEM((rows, wide), bf16),
            pltpu.VMEM((rows, n * rows), jnp.float32),
            pltpu.VMEM((2, rows, wide), bf16),
            dma((5,)),
            dma((5 * 5 * n,)),
            dma((5 * 5 * n,)),
            dma((n - 1,)),
            dma((n - 1,)),
            dma,
            dma,
        ],
        compiler_params=pltpu.CompilerParams(
            collective_id=0, has_side_effects=True, vmem_limit_bytes=56 * 2**20
        ),
    )(chosen, live_length, tokens, query_weight, key_weight, value_weight, out_weight)


def solution(mesh):
    in_specs = (
        P(("dp", "kv"), None),
        P("kv", "tp"),
        P("kv", "tp"),
        P("kv", "tp"),
        P("kv", "tp"),
        P(("dp", "kv"), None),
        P("dp"),
    )
    out_specs = P(("dp", "kv"), "tp")
    fits = (mesh.shape["dp"], mesh.shape["kv"], mesh.shape["tp"]) == (4, 4, 2)
    body = woven_body if fits else gathered_body
    return jax.shard_map(body, mesh=mesh, in_specs=in_specs, out_specs=out_specs, check_vma=False)
```

profile of v0, /device:TPU:0, one launch (start us, length us, event | category | flops | bytes accessed | tf_op | source)
XLA Modules:
  0.0 83.5 jit_solution(12765777763426688900)
XLA Ops:
  0.7 80.6 %shard_map.73 = bf16[256,2048]{1,0:T(8,128)(2,1)} custom-call(s32[8,16]{1,0:T(8,128)} %chosen.1, s32[1]{0:T(128)S(6)} %copy.9.live, bf16[256,4096]{1,0:T(8,128)(2,1)} %tokens.1, bf16[1024,512]{1,0:T(8,128)(2,1)} %query_w.1, bf16[1024,128]{1,0:T(8,128)(2,1)} %key_w.1, bf16[1024,128]{1,0:T(8,128)(2,1)} %value_w.1, bf16[256,2048]{1,0:T(8,128)(2,1)} %out_w.1), custom_call_target="tpu_custom_call" | custom-call | tf_op jit(solution)/shard_map/pallas_call | solution.py:372
  81.2 2.3 %copy.10 = bf16[256,2048]{1,0:T(8,128)(2,1)} copy(bf16[256,2048]{1,0:T(8,128)(2,1)} %shard_map.73) | data formatting | bytes 2097152
where the time goes:
time: 83.7 us; the launch traced here: 83.5 us
  Pallas kernels  80.6 us (96%)
  local copies, waits for them, and re-layouts  2.3 us (3%)
    pallas_call x1, Pallas kernels, woven_body(): pl.pallas_call(functools.partial(kernel, n), out_shape=jax.ShapeDtypeStru...  80.6 us
    unnamed x1, local copies, waits for them, and re-layouts  2.3 us

commit v1 on v0

v1 whole, which is shorter than its diff:
```python
import functools

import jax
import jax.numpy as jnp
from jax import lax
from jax.experimental import pallas as pl
from jax.experimental.pallas import tpu as pltpu
from jax.sharding import PartitionSpec as P

HD = 128
BLOCK = 32
CAP = 2
MESH = pl.DeviceIdType.MESH


def gathered_body(tokens, query_weight, key_weight, value_weight, out_weight, chosen, live_length):
    rows = tokens.shape[0]
    per_dev = rows // BLOCK
    owners = lax.axis_size("kv")
    me = lax.axis_index("kv")

    def add_rows(piece):
        return jnp.dot(tokens, piece, preferred_element_type=jnp.float32)

    queries = add_rows(lax.all_gather(query_weight, "kv", axis=0, tiled=True))
    keys = add_rows(lax.all_gather(key_weight, "kv", axis=0, tiled=True))
    values = add_rows(lax.all_gather(value_weight, "kv", axis=0, tiled=True))
    queries = queries.astype(jnp.bfloat16)
    paired = jnp.concatenate([keys.astype(jnp.bfloat16), values.astype(jnp.bfloat16)], axis=1)
    width = paired.shape[1]
    local_blocks = paired.reshape(per_dev, BLOCK, width)
    valid = chosen >= 0
    safe = jnp.maximum(chosen, 0)
    blocks_all = owners * per_dev
    hits = (safe[:, :, None] == jnp.arange(blocks_all, dtype=jnp.int32)[None, None, :]) & valid[
        :, :, None
    ]
    needed = jnp.any(hits, axis=(0, 1)).reshape(owners, per_dev)
    needed = needed & (jnp.arange(owners, dtype=jnp.int32) != me)[:, None]
    ranks = jnp.cumsum(needed.astype(jnp.int32), axis=1)
    local_ids = jnp.arange(per_dev, dtype=jnp.int32)
    slot_lists = []
    for slot in range(CAP):
        marked = needed & (ranks == slot + 1)
        found = jnp.any(marked, axis=1)
        where_at = jnp.sum(jnp.where(marked, local_ids[None, :], 0), axis=1)
        slot_lists.append(jnp.where(found, where_at, -1))
    wanted = jnp.stack(slot_lists, axis=1)
    requested = lax.all_to_all(wanted, "kv", split_axis=0, concat_axis=0, tiled=True)
    outgoing = local_blocks[jnp.maximum(requested, 0)]
    outgoing = jnp.where((requested >= 0)[:, :, None, None], outgoing, jnp.zeros((), jnp.bfloat16))
    incoming = lax.all_to_all(outgoing, "kv", split_axis=0, concat_axis=0, tiled=True)
    table = jnp.concatenate([incoming.reshape(owners * CAP, BLOCK, width), local_blocks], axis=0)
    segment_retainer = safe // per_dev
    local_of = safe % per_dev
    match = (wanted[None, None, :, :] == local_of[:, :, None, None]) & (
        jnp.arange(owners, dtype=jnp.int32)[None, None, :, None]
        == segment_retainer[:, :, None, None]
    )
    slot_index = jnp.arange(owners * CAP, dtype=jnp.int32).reshape(owners, CAP)
    remote_at = jnp.sum(jnp.where(match, slot_index[None, None], 0), axis=(2, 3))
    position = jnp.where(segment_retainer == me, owners * CAP + local_of, remote_at)
    picked = table[position]
    near_keys = picked[..., :HD]
    near_values = picked[..., HD:]
    grouped = queries.reshape(per_dev, BLOCK, -1, HD)
    scores = jnp.einsum(
        "jqhd,jnbd->jhqnb", grouped, near_keys, preferred_element_type=jnp.float32
    ) * HD ** (-0.5)
    query_pos = (me * per_dev + jnp.arange(per_dev, dtype=jnp.int32))[:, None] * BLOCK + jnp.arange(
        BLOCK, dtype=jnp.int32
    )[None, :]
    key_pos = safe[:, :, None] * BLOCK + jnp.arange(BLOCK, dtype=jnp.int32)[None, None, :]
    allowed = valid[:, None, :, None] & (key_pos[:, None, :, :] <= query_pos[:, :, None, None])
    masked = jnp.where(allowed[:, None], scores, -jnp.inf)
    top = jnp.max(masked, axis=(3, 4), keepdims=True)
    weights = jnp.exp(masked - top)
    total = jnp.sum(weights, axis=(3, 4))
    summed = jnp.einsum(
        "jhqnb,jnbd->jqhd",
        weights.astype(jnp.bfloat16),
        near_values,
        preferred_element_type=jnp.float32,
    )
    result = summed / jnp.transpose(total, (0, 2, 1))[..., None]
    live = query_pos < live_length[0]
    result = jnp.where(live[:, :, None, None], result, 0.0)
    attended = result.astype(jnp.bfloat16).reshape(rows, -1)
    every_head = lax.all_gather(attended, "tp", axis=1, tiled=True)
    mixed = jnp.dot(
        every_head,
        lax.all_gather(out_weight, "kv", axis=0, tiled=True),
        preferred_element_type=jnp.float32,
    )
    return mixed.astype(jnp.bfloat16)


HALF = 2
MODES = "qqqh"
ORDER = (
    ("own", 0), ("own", 1), ("own", 2), ("w", 0), ("t", 0), ("w", 1), ("t", 1), ("w", 2),
    ("own", 0, "o"), ("t", 2), ("w", 3), ("t", 3), ("w", 4), ("own", 1, "o"), ("w", 5), ("w", 6),
    ("own", 2, "o"), ("w", 7), ("o", 0, 0), ("kv1",), ("o", 0, 1), ("oc", 0, 0), ("w", 8),
    ("own", 3, "o"), ("kv2",), ("oc", 0, 1), ("o", 0, 2), ("q1", 0), ("q1", 1), ("oc", 0, 2),
    ("o", 1, 0), ("o", 1, 1), ("oc", 1, 0), ("q2", 0), ("o", 1, 2), ("oc", 1, 1), ("q2", 1),
    ("o", 2, 0), ("oc", 1, 2), ("o", 2, 1), ("att", 2, 0), ("oc", 2, 0), ("o", 2, 2),
    ("oc", 2, 1), ("att", 2, 1), ("share",), ("o", 3, 0), ("oc", 2, 2), ("o", 3, 1), ("o", 3, 2),
    ("fin", 0), ("fin", 1), ("fin", 2), ("oc", 3, 0), ("oc", 3, 1), ("oc", 3, 2), ("fin", 3),
)


def pick(at, values):
    out = jnp.int32(values[0])
    for i, v in enumerate(values[1:]):
        out = jnp.where(at == i + 1, jnp.int32(v), out)
    return out


class Mover:
    def __init__(self, sends, recvs):
        self.sends, self.recvs = sends, recvs
        self.begun = []

    def copy(self, src, dst, send, recv, target):
        return pltpu.make_async_remote_copy(
            src_ref=src, dst_ref=dst, send_sem=self.sends.at[send], recv_sem=self.recvs.at[recv],
            device_id=target, device_id_type=MESH,
        )

    def begin(self, c, when=None):
        if when is None:
            c.start()
        else:
            pl.when(when)(c.start)
        self.begun.append((c, when))

    def finish(self):
        for c, when in self.begun:
            if when is None:
                c.wait_send()
            else:
                pl.when(when)(c.wait_send)


def kernel(
    n, chosen, live, tokens, query_w, key_w, value_w, out_w, listing, mixed,
    tok, other, weights, outs, lists, table, picked, mine_kv, mine_q, away, back,
    queries, bias, attended, staged, local_sem, send_sem, recv_sem, out_sem,
):
    dp, me, tp = lax.axis_index("dp"), lax.axis_index("kv"), lax.axis_index("tp")
    x_at, y_at = lax.rem(dp, 2), lax.div(dp, 2)
    right, left = jnp.minimum(me + 1, n - 1), jnp.maximum(me - 1, 0)
    to_x = {"dp": 2 * y_at + (1 - x_at)}
    to_y = {"dp": 2 * (1 - y_at) + x_at}
    dp_x, dp_y = 2 * y_at + (1 - x_at), 2 * (1 - y_at) + x_at
    dp_far = 2 * (1 - y_at) + (1 - x_at)
    side = lax.rem(x_at + y_at, 2)
    partner = {"tp": 1 - tp}
    rows = other.shape[0]
    depth = tok.shape[1]
    per_dev = rows // BLOCK
    seg = depth // n
    half_seg = seg // 2
    width = weights.shape[1]
    groups = weights.shape[0] // depth
    owned = outs.shape[0] // len(MODES) // n
    tall = n * owned
    tile = outs.shape[1]
    is_end = jnp.logical_or(me == 0, me == n - 1)
    near = [pick(me, v) for v in ((1, 2, 1, 2), (2, 0, 3, 1), (3, 3, 0, 0))]
    mover = Mover(send_sem, recv_sem)

    loads = []

    def load(src, dst):
        c = pltpu.make_async_copy(src, dst, local_sem.at[len(loads)])
        c.start()
        loads.append(c)
        return c

    my_rows = pl.ds(pl.multiple_of(x_at * seg, seg), seg)

    def slab(group):
        return pl.ds(pl.multiple_of(group * depth + me * seg, seg), seg)

    kv_load = [
        load(key_w.at[my_rows, :], weights.at[slab(0), :HD]),
        load(value_w.at[my_rows, :], weights.at[slab(0), HD:]),
    ]
    q_load = [
        load(query_w.at[my_rows, i * width : (i + 1) * width], weights.at[slab(1 + i), :])
        for i in range(groups - 1)
    ]
    tok_load = [
        load(
            tokens.at[:, pl.ds(pl.multiple_of((2 * k + x_at) * seg, seg), seg)],
            tok.at[:, k * seg : (k + 1) * seg],
        )
        for k in range(n)
    ]
    o_load = [
        load(
            out_w.at[:, s * tile : (s + 1) * tile],
            outs.at[pl.ds(pl.multiple_of(s * tall + me * owned, owned), owned), :],
        )
        for s in range(len(MODES))
    ]
    list_load = load(listing, lists.at[me])

    barrier = pltpu.get_barrier_semaphore()
    greeted = [{"kv": lax.rem(me + step, n)} for step in range(1, n)] + [to_x, to_y, partner]
    for target in greeted:
        pl.semaphore_signal(barrier, inc=1, device_id=target, device_id_type=MESH)
    pl.semaphore_wait(barrier, len(greeted))

    W = 0
    O = W + groups * n * 3
    T = O + len(MODES) * n * 6
    L = T + 2 * n
    K = L + n
    Y = K + n
    S = Y + groups

    my_part = pl.ds(pl.multiple_of(tp * (rows // 2), rows // 2), rows // 2)
    their_part = pl.ds(pl.multiple_of((1 - tp) * (rows // 2), rows // 2), rows // 2)

    def t_copy(k):
        cols = pl.ds(pl.multiple_of((2 * k + 1 - x_at) * seg, seg), seg)
        return mover.copy(
            tokens.at[my_part, cols], other.at[my_part, k * seg : (k + 1) * seg], T + k, T + k, to_x
        )

    def t_share(k, part):
        piece = other.at[part, k * seg : (k + 1) * seg]
        return mover.copy(piece, piece, T + n + k, T + n + k, partner)

    for k in range(n):
        mover.begin(t_copy(k))

    def l_copy(step):
        return mover.copy(
            listing, lists.at[me], L + step, L + step, {"kv": jnp.maximum(me - step, 0)}
        )

    for step in range(1, n):
        mover.begin(l_copy(step), me >= step)

    def w_piece(group, owner, which):
        start = group * depth + owner * seg + which * half_seg
        return weights.at[pl.ds(pl.multiple_of(start, half_seg), half_seg), :]

    def w_copy(group, owner, which, kind, target, sent=None):
        at = W + (group * n + owner) * 3
        piece = w_piece(group, owner, which)
        return mover.copy(piece, piece, at + (kind if sent is None else sent), at + kind, target)

    def w_own(group):
        for c in (kv_load if group == 0 else q_load[group - 1 : group]):
            c.wait()
        mover.begin(w_copy(group, me, y_at, 0, {"kv": right}), me < n - 1)
        mover.begin(w_copy(group, me, y_at, 0, {"kv": left}, 2), me > 0)

    def w_step(p):
        inner = (p // 2, p % 2) if p < 2 * groups else (p - 2 * groups, 2)
        group = jnp.where(is_end, p % groups, inner[0])
        owner = jnp.where(is_end, near[p // groups], near[inner[1]])
        w_copy(group, owner, y_at, 0, {"kv": right}).wait_recv()
        mover.begin(
            w_copy(group, owner, y_at, 0, {"kv": right}), jnp.logical_and(owner < me, me < n - 1)
        )
        mover.begin(w_copy(group, owner, y_at, 0, {"kv": left}), jnp.logical_and(owner > me, me > 0))
        mover.begin(w_copy(group, owner, y_at, 1, to_y))

    def w_arrive(group):
        for owner in near:
            w_copy(group, owner, 1 - y_at, 1, to_y).wait_recv()

    def o_piece(s, owner, index, count):
        size = owned // count
        return outs.at[
            pl.ds(pl.multiple_of(s * tall + owner * owned + index * size, size), size), :
        ]

    def o_copy(s, owner, index, count, kind, target, sent=None):
        at = O + (s * n + owner) * 6
        piece = o_piece(s, owner, index, count)
        return mover.copy(piece, piece, at + (kind if sent is None else sent), at + kind, target)

    def o_carried(s, owner):
        return (s, owner, dp, 4) if MODES[s] == "q" else (s, owner, side, 2)

    def o_own(s):
        o_load[s].wait()
        mover.begin(o_copy(*o_carried(s, me), 0, {"kv": right}), me < n - 1)
        mover.begin(o_copy(*o_carried(s, me), 0, {"kv": left}, 5), me > 0)

    def o_step(s, slot):
        owner = near[slot]
        carried = o_carried(s, owner)
        o_copy(*carried, 0, {"kv": right}).wait_recv()
        mover.begin(o_copy(*carried, 0, {"kv": right}), jnp.logical_and(owner < me, me < n - 1))
        mover.begin(o_copy(*carried, 0, {"kv": left}), jnp.logical_and(owner > me, me > 0))
        if MODES[s] == "q":
            mover.begin(o_copy(*carried, 1, to_x))
            mover.begin(o_copy(*carried, 2, to_y))
        else:
            mover.begin(o_copy(s, owner, 2 * side, 4, 1, to_x))
            mover.begin(o_copy(s, owner, 2 * side + 1, 4, 2, to_y))

    def o_corner(s, slot):
        owner = near[slot]
        if MODES[s] == "q":
            o_copy(s, owner, dp_x, 4, 1, to_x).wait_recv()
            mover.begin(o_copy(s, owner, 2 * dp_x, 8, 4, to_y))
            o_copy(s, owner, dp_y, 4, 2, to_y).wait_recv()
            mover.begin(o_copy(s, owner, 2 * dp_y + 1, 8, 3, to_x))
        else:
            o_copy(s, owner, 2 * (1 - side), 4, 1, to_x).wait_recv()
            o_copy(s, owner, 2 * (1 - side) + 1, 4, 2, to_y).wait_recv()

    def o_arrive(s):
        if MODES[s] == "q":
            for owner in near:
                o_copy(s, owner, 2 * dp_far, 8, 4, to_y).wait_recv()
                o_copy(s, owner, 2 * dp_far + 1, 8, 3, to_x).wait_recv()

    def part(source, group):
        return jnp.dot(
            source[...], weights[group * depth : (group + 1) * depth, :],
            preferred_element_type=jnp.float32,
        )

    def y_copy(group):
        return mover.copy(away.at[group], back.at[group], Y + group, Y + group, to_x)

    def project(group):
        w_arrive(group)
        away[group] = part(other, group).astype(jnp.bfloat16)
        mover.begin(y_copy(group))
        if group == 0:
            mine_kv[...] = part(tok, group)
        else:
            mine_q[:, (group - 1) * width : group * width] = part(tok, group)

    slots = CAP * BLOCK
    local_at = n * slots

    def found(listed, block):
        return jnp.max((listed == block).astype(jnp.float32), axis=(0, 1), keepdims=True)

    def marks(listed, first):
        rank = jnp.zeros((1, 1), jnp.float32)
        out = [[] for _ in range(CAP)]
        for b in range(per_dev):
            one = found(listed, first + b)
            rank = rank + one
            for s in range(CAP):
                out[s].append(jnp.where(rank == s + 1, one, 0.0))
        return out

    def k_copy(step):
        return mover.copy(
            picked.at[step - 1], table.at[pl.ds(pl.multiple_of(me * slots, slots), slots), :],
            K + step, K + step, {"kv": jnp.minimum(me + step, n - 1)},
        )

    def k_arrive():
        for step in range(1, n):
            owner = jnp.maximum(me - step, 0)
            c = mover.copy(
                picked.at[step - 1],
                table.at[pl.ds(pl.multiple_of(owner * slots, slots), slots), :],
                K + step, K + step, {"kv": jnp.minimum(me + step, n - 1)},
            )
            pl.when(me >= step)(c.wait_recv)

    def share_blocks():
        y_copy(0).wait_recv()
        full = (mine_kv[...] + back[0].astype(jnp.float32)).astype(jnp.bfloat16)
        table[local_at : local_at + rows, :] = full
        full = full.astype(jnp.float32)
        for step in range(1, n):
            pl.when(me + step < n)(l_copy(step).wait_recv)
        for step in range(1, n):

            def send_to(step=step):
                which = marks(lists[me + step], me * per_dev)
                for s in range(CAP):
                    kept = jnp.zeros((BLOCK, full.shape[1]), jnp.float32)
                    for b in range(per_dev):
                        kept = kept + which[s][b] * full[b * BLOCK : (b + 1) * BLOCK, :]
                    picked[step - 1, s * BLOCK : (s + 1) * BLOCK, :] = kept.astype(jnp.bfloat16)

            pl.when(me + step < n)(send_to)
            mover.begin(k_copy(step), me + step < n)

    def build_bias():
        list_load.wait()
        listed = lists[me]
        seq = bias.shape[1]
        column = lax.broadcasted_iota(jnp.int32, (8, seq), 1)
        block = me * per_dev + lax.div(column - local_at, BLOCK)
        for owner in range(n):
            which = marks(listed, owner * per_dev)
            for s in range(CAP):
                ident = jnp.full((1, 1), -2.0, jnp.float32)
                for b in range(per_dev):
                    ident = jnp.where(which[s][b] > 0.5, float(owner * per_dev + b), ident)
                ident = jnp.where(me == owner, -2.0, ident).astype(jnp.int32)
                block = jnp.where(lax.div(column, BLOCK) == owner * CAP + s, ident, block)
        at = block * BLOCK + lax.rem(column, BLOCK)
        at = jnp.concatenate([at] * (BLOCK // 8), axis=0)
        row = lax.broadcasted_iota(jnp.int32, (BLOCK, seq), 0)
        for j in range(per_dev):
            open_to = jnp.full((8, seq), -jnp.inf, jnp.float32)
            for e in range(chosen.shape[1]):
                open_to = jnp.where(block == chosen[j, e], 0.0, open_to)
            spread = jnp.concatenate([open_to] * (BLOCK // 8), axis=0)
            causal = at <= row + (me * rows + j * BLOCK)
            bias[j * BLOCK : (j + 1) * BLOCK, :] = jnp.where(causal, spread, -jnp.inf)

    def queries_done(half):
        y_copy(1 + half).wait_recv()
        cols = slice(half * width, (half + 1) * width)
        queries[:, cols] = (
            mine_q[:, cols] + back[1 + half].astype(jnp.float32)
        ).astype(jnp.bfloat16)

    def attend(count, index):
        if index == 0:
            k_arrive()
        alive = me * rows + lax.broadcasted_iota(jnp.int32, (rows, HD), 0) < live[0]
        for h in range(count * index, count * (index + 1)):
            cols = slice(h * HD, (h + 1) * HD)
            scores = lax.dot_general(
                queries[:, cols], table[:, :HD], (((1,), (1,)), ((), ())),
                preferred_element_type=jnp.float32,
            )
            masked = scores * HD ** (-0.5) + bias[...]
            top = jnp.max(masked, axis=1, keepdims=True)
            probs = jnp.exp(masked - top)
            total = jnp.sum(probs, axis=1, keepdims=True)
            summed = jnp.dot(
                probs.astype(jnp.bfloat16), table[:, HD:], preferred_element_type=jnp.float32
            )
            attended[tp, :, cols] = jnp.where(alive, summed / total, 0.0).astype(jnp.bfloat16)

    def share_copy(at):
        return mover.copy(attended.at[at], attended.at[at], S, S, partner)

    wide = queries.shape[1]
    stores = []
    shared = []

    def final(s):
        if not shared:
            share_copy(1 - tp).wait_recv()
            shared.append(True)
        o_arrive(s)
        acc = jnp.dot(
            attended[0], outs[s * tall : s * tall + wide, :], preferred_element_type=jnp.float32
        )
        acc += jnp.dot(
            attended[1], outs[s * tall + wide : (s + 1) * tall, :],
            preferred_element_type=jnp.float32,
        )
        staged[s] = acc.astype(jnp.bfloat16)
        c = pltpu.make_async_copy(
            staged.at[s], mixed.at[:, s * tile : (s + 1) * tile], out_sem.at[s]
        )
        c.start()
        stores.append(c)

    shared_out = []
    built = []
    for step in ORDER:
        name, args = step[0], step[1:]
        if name == "own":
            o_own(args[0]) if len(args) > 1 else w_own(args[0])
        elif name == "w":
            if not built:
                for owner in range(n):
                    def clear(owner=owner):
                        table[owner * slots : (owner + 1) * slots, :] = jnp.zeros(
                            (slots, table.shape[1]), table.dtype
                        )
                    pl.when(owner >= me)(clear)
                build_bias()
                for c in tok_load:
                    c.wait()
                built.append(True)
            w_step(args[0])
        elif name == "t":
            t_copy(args[0]).wait_recv()
            mover.begin(t_share(args[0], my_part))
        elif name == "o":
            o_step(*args)
        elif name == "oc":
            o_corner(*args)
        elif name == "kv1":
            for k in range(n):
                t_share(k, their_part).wait_recv()
            project(0)
        elif name == "q1":
            project(1 + args[0])
        elif name == "kv2":
            share_blocks()
        elif name == "q2":
            queries_done(args[0])
        elif name == "att":
            attend(*args)
        elif name == "share":
            c = share_copy(tp)
            mover.begin(c)
        else:
            final(args[0])
    mover.finish()
    for c in stores:
        c.wait()


def woven_body(tokens, query_weight, key_weight, value_weight, out_weight, chosen, live_length):
    n = lax.axis_size("kv")
    rows, model = tokens.shape
    wide = query_weight.shape[1]
    depth = model // HALF
    width = 2 * HD
    groups = 1 + wide // width
    chunks = len(MODES)
    tile = out_weight.shape[1] // chunks
    slots = CAP * BLOCK
    total = n * slots + rows
    dma = pltpu.SemaphoreType.DMA
    bf16 = jnp.bfloat16
    f32 = jnp.float32
    anywhere = pl.BlockSpec(memory_space=pl.ANY)
    small = pl.BlockSpec(memory_space=pltpu.SMEM)
    sems = groups * n * 3 + chunks * n * 6 + 2 * n + n + n + groups + 1
    return pl.pallas_call(
        functools.partial(kernel, n),
        out_shape=jax.ShapeDtypeStruct((rows, out_weight.shape[1]), bf16),
        in_specs=[small, small] + [anywhere] * 6,
        out_specs=anywhere,
        scratch_shapes=[
            pltpu.VMEM((rows, depth), bf16),
            pltpu.VMEM((rows, depth), bf16),
            pltpu.VMEM((groups * depth, width), bf16),
            pltpu.VMEM((chunks * n * out_weight.shape[0], tile), bf16),
            pltpu.VMEM((n,) + chosen.shape, jnp.int32),
            pltpu.VMEM((total, width), bf16),
            pltpu.VMEM((n - 1, slots, width), bf16),
            pltpu.VMEM((rows, width), f32),
            pltpu.VMEM((rows, wide), f32),
            pltpu.VMEM((groups, rows, width), bf16),
            pltpu.VMEM((groups, rows, width), bf16),
            pltpu.VMEM((rows, wide), bf16),
            pltpu.VMEM((rows, total), f32),
            pltpu.VMEM((2, rows, wide), bf16),
            pltpu.VMEM((chunks, rows, tile), bf16),
            dma((2 + groups - 1 + n + chunks + 1,)),
            dma((sems,)),
            dma((sems,)),
            dma((chunks,)),
        ],
        compiler_params=pltpu.CompilerParams(
            collective_id=0, has_side_effects=True, vmem_limit_bytes=48 * 2**20
        ),
    )(chosen, live_length, tokens, query_weight, key_weight, value_weight, out_weight, chosen)


def solution(mesh):
    in_specs = (
        P(("dp", "kv"), None),
        P("kv", "tp"),
        P("kv", "tp"),
        P("kv", "tp"),
        P("kv", "tp"),
        P(("dp", "kv"), None),
        P("dp"),
    )
    out_specs = P(("dp", "kv"), "tp")
    fits = (mesh.shape["dp"], mesh.shape["kv"], mesh.shape["tp"]) == (4, 4, 2)
    body = woven_body if fits else gathered_body
    return jax.shard_map(body, mesh=mesh, in_specs=in_specs, out_specs=out_specs, check_vma=False)
```

time: 83.7 us -> 86.1 us (1.029)
  local copies, waits for them, and re-layouts: 2.3 us -> 7.59 us
  Pallas kernels: 80.6 us -> 77.5 us
    unnamed x1 -> x13, local copies, waits for them, and re-layouts: 2.3 us -> 7.59 us
    pallas_call x1, Pallas kernels: 80.6 us -> 77.5 us  [woven_body(): pl.pallas_call(functools.partial(kernel, n), out_shape=jax.ShapeDtypeStru...]
where the time goes in v1:
time: 86.1 us; the launch traced here: 85.8 us
  Pallas kernels  77.5 us (90%)
  local copies, waits for them, and re-layouts  7.59 us (9%)
    pallas_call x1, Pallas kernels, woven_body(): pl.pallas_call(functools.partial(kernel, n), out_shape=jax.ShapeDtypeStru...  77.5 us
    unnamed x13, local copies, waits for them, and re-layouts  7.59 us

profile of v1, /device:TPU:0, one launch (start us, length us, event | category | flops | bytes accessed | tf_op | source)
XLA Modules:
  0.0 85.8 jit_solution(4048141126322353032)
XLA Ops:
  0.7 0.0 copy-start
  0.7 1.6 %copy-done = bf16[256,4096]{1,0:T(8,128)(2,1)S(1)} copy-done((bf16[256,4096]{1,0:T(8,128)(2,1)S(1)}, bf16[256,4096]{1,0:T(8,128)(2,1)}, u32[]{:S(2)}) %copy-start) | copy-done | bytes 2097176
  2.2 0.0 copy-start.1
  2.2 1.2 %copy-done.1 = bf16[1024,512]{1,0:T(8,128)(2,1)S(1)} copy-done((bf16[1024,512]{1,0:T(8,128)(2,1)S(1)}, bf16[1024,512]{1,0:T(8,128)(2,1)}, u32[]{:S(2)}) %copy-start.1) | copy-done | bytes 1048600
  3.5 0.0 copy-start.2
  3.5 1.2 %copy-done.2 = bf16[256,2048]{1,0:T(8,128)(2,1)S(1)} copy-done((bf16[256,2048]{1,0:T(8,128)(2,1)S(1)}, bf16[256,2048]{1,0:T(8,128)(2,1)}, u32[]{:S(2)}) %copy-start.2) | copy-done | bytes 1048600
  4.7 0.0 copy-start.3
  4.7 0.9 %copy-done.3 = bf16[1024,128]{1,0:T(8,128)(2,1)S(1)} copy-done((bf16[1024,128]{1,0:T(8,128)(2,1)S(1)}, bf16[1024,128]{1,0:T(8,128)(2,1)}, u32[]{:S(2)}) %copy-start.3) | copy-done | bytes 262168
  5.6 0.0 copy-start.4
  5.6 0.9 %copy-done.4 = bf16[1024,128]{1,0:T(8,128)(2,1)S(1)} copy-done((bf16[1024,128]{1,0:T(8,128)(2,1)S(1)}, bf16[1024,128]{1,0:T(8,128)(2,1)}, u32[]{:S(2)}) %copy-start.4) | copy-done | bytes 262168
  6.6 0.0 copy-start.5
  6.6 0.7 copy-done.5
  7.3 77.5 %shard_map.73 = bf16[256,2048]{1,0:T(8,128)(2,1)S(1)} custom-call(s32[8,16]{1,0:T(8,128)S(1)} %copy-done.5, s32[1]{0:T(128)S(6)} %copy.9.live, bf16[256,4096]{1,0:T(8,128)(2,1)S(1)} %copy-done, bf16[1024,512]{1,0:T(8,128)(2,1)S(1)} %copy-done.1, bf16[1024,128]{1,0:T(8,128)(2,1)S(1)} %copy-done.3, bf16[1024,128]{1,0:T(8,128)(2,1)S(1)} %copy-done.4, ...), custom_call_target="tpu_custom_call" | custom-call | tf_op jit(solution)/shard_map/pallas_call | solution.py:539
  84.8 1.0 %copy.10 = bf16[256,2048]{1,0:T(8,128)(2,1)} copy(bf16[256,2048]{1,0:T(8,128)(2,1)S(1)} %shard_map.73) | data formatting | bytes 2097152
Async XLA Ops:
  0.7 1.6 %copy-start = (bf16[256,4096]{1,0:T(8,128)(2,1)S(1)}, bf16[256,4096]{1,0:T(8,128)(2,1)}, u32[]{:S(2)}) copy-start(bf16[256,4096]{1,0:T(8,128)(2,1)} %tokens.1) | copy-start | bytes 6291460
  2.2 1.2 %copy-start.1 = (bf16[1024,512]{1,0:T(8,128)(2,1)S(1)}, bf16[1024,512]{1,0:T(8,128)(2,1)}, u32[]{:S(2)}) copy-start(bf16[1024,512]{1,0:T(8,128)(2,1)} %query_w.1) | copy-start | bytes 3145732
  3.5 1.2 %copy-start.2 = (bf16[256,2048]{1,0:T(8,128)(2,1)S(1)}, bf16[256,2048]{1,0:T(8,128)(2,1)}, u32[]{:S(2)}) copy-start(bf16[256,2048]{1,0:T(8,128)(2,1)} %out_w.1) | copy-start | bytes 3145732
  4.7 0.9 %copy-start.3 = (bf16[1024,128]{1,0:T(8,128)(2,1)S(1)}, bf16[1024,128]{1,0:T(8,128)(2,1)}, u32[]{:S(2)}) copy-start(bf16[1024,128]{1,0:T(8,128)(2,1)} %key_w.1) | copy-start | bytes 786436
  5.6 0.9 %copy-start.4 = (bf16[1024,128]{1,0:T(8,128)(2,1)S(1)}, bf16[1024,128]{1,0:T(8,128)(2,1)}, u32[]{:S(2)}) copy-start(bf16[1024,128]{1,0:T(8,128)(2,1)} %value_w.1) | copy-start | bytes 786436
  6.6 0.7 copy-start.5

commit v2 on v1

v2 whole, which is shorter than its diff:
```python
import functools
import math

import jax
import jax.numpy as jnp
from jax import lax
from jax.experimental import pallas as pl
from jax.experimental.pallas import tpu as pltpu
from jax.sharding import PartitionSpec as P

HD = 128
BLOCK = 32
CAP = 2
MESH = pl.DeviceIdType.MESH


def gathered_body(tokens, query_weight, key_weight, value_weight, out_weight, chosen, live_length):
    rows = tokens.shape[0]
    per_dev = rows // BLOCK
    owners = lax.axis_size("kv")
    me = lax.axis_index("kv")

    def add_rows(piece):
        return jnp.dot(tokens, piece, preferred_element_type=jnp.float32)

    queries = add_rows(lax.all_gather(query_weight, "kv", axis=0, tiled=True))
    keys = add_rows(lax.all_gather(key_weight, "kv", axis=0, tiled=True))
    values = add_rows(lax.all_gather(value_weight, "kv", axis=0, tiled=True))
    queries = queries.astype(jnp.bfloat16)
    paired = jnp.concatenate([keys.astype(jnp.bfloat16), values.astype(jnp.bfloat16)], axis=1)
    width = paired.shape[1]
    local_blocks = paired.reshape(per_dev, BLOCK, width)
    valid = chosen >= 0
    safe = jnp.maximum(chosen, 0)
    blocks_all = owners * per_dev
    hits = (safe[:, :, None] == jnp.arange(blocks_all, dtype=jnp.int32)[None, None, :]) & valid[
        :, :, None
    ]
    needed = jnp.any(hits, axis=(0, 1)).reshape(owners, per_dev)
    needed = needed & (jnp.arange(owners, dtype=jnp.int32) != me)[:, None]
    ranks = jnp.cumsum(needed.astype(jnp.int32), axis=1)
    local_ids = jnp.arange(per_dev, dtype=jnp.int32)
    slot_lists = []
    for slot in range(CAP):
        marked = needed & (ranks == slot + 1)
        found = jnp.any(marked, axis=1)
        where_at = jnp.sum(jnp.where(marked, local_ids[None, :], 0), axis=1)
        slot_lists.append(jnp.where(found, where_at, -1))
    wanted = jnp.stack(slot_lists, axis=1)
    requested = lax.all_to_all(wanted, "kv", split_axis=0, concat_axis=0, tiled=True)
    outgoing = local_blocks[jnp.maximum(requested, 0)]
    outgoing = jnp.where((requested >= 0)[:, :, None, None], outgoing, jnp.zeros((), jnp.bfloat16))
    incoming = lax.all_to_all(outgoing, "kv", split_axis=0, concat_axis=0, tiled=True)
    table = jnp.concatenate([incoming.reshape(owners * CAP, BLOCK, width), local_blocks], axis=0)
    segment_retainer = safe // per_dev
    local_of = safe % per_dev
    match = (wanted[None, None, :, :] == local_of[:, :, None, None]) & (
        jnp.arange(owners, dtype=jnp.int32)[None, None, :, None]
        == segment_retainer[:, :, None, None]
    )
    slot_index = jnp.arange(owners * CAP, dtype=jnp.int32).reshape(owners, CAP)
    remote_at = jnp.sum(jnp.where(match, slot_index[None, None], 0), axis=(2, 3))
    position = jnp.where(segment_retainer == me, owners * CAP + local_of, remote_at)
    picked = table[position]
    near_keys = picked[..., :HD]
    near_values = picked[..., HD:]
    grouped = queries.reshape(per_dev, BLOCK, -1, HD)
    scores = jnp.einsum(
        "jqhd,jnbd->jhqnb", grouped, near_keys, preferred_element_type=jnp.float32
    ) * HD ** (-0.5)
    query_pos = (me * per_dev + jnp.arange(per_dev, dtype=jnp.int32))[:, None] * BLOCK + jnp.arange(
        BLOCK, dtype=jnp.int32
    )[None, :]
    key_pos = safe[:, :, None] * BLOCK + jnp.arange(BLOCK, dtype=jnp.int32)[None, None, :]
    allowed = valid[:, None, :, None] & (key_pos[:, None, :, :] <= query_pos[:, :, None, None])
    masked = jnp.where(allowed[:, None], scores, -jnp.inf)
    top = jnp.max(masked, axis=(3, 4), keepdims=True)
    weights = jnp.exp(masked - top)
    total = jnp.sum(weights, axis=(3, 4))
    summed = jnp.einsum(
        "jhqnb,jnbd->jqhd",
        weights.astype(jnp.bfloat16),
        near_values,
        preferred_element_type=jnp.float32,
    )
    result = summed / jnp.transpose(total, (0, 2, 1))[..., None]
    live = query_pos < live_length[0]
    result = jnp.where(live[:, :, None, None], result, 0.0)
    attended = result.astype(jnp.bfloat16).reshape(rows, -1)
    every_head = lax.all_gather(attended, "tp", axis=1, tiled=True)
    mixed = jnp.dot(
        every_head,
        lax.all_gather(out_weight, "kv", axis=0, tiled=True),
        preferred_element_type=jnp.float32,
    )
    return mixed.astype(jnp.bfloat16)


HALF = 2
LEAST = 16
CUTS = {"q": 32, "p": 16}
MODES = "ppph"
WEIGHTS, OUTS, REST = range(3)
BULK = 3
ORDER_END = (
    ("owno", 1, 0), ("own", 0, 0), ("owno", 0, 0), ("owno", 2, 0), ("own", 1, 0), ("o", 0, 0),
    ("own", 2, 0), ("o", 1, 0), ("o", 2, 0), ("o", 0, 1), ("w", 0, 0), ("o", 2, 1), ("o", 1, 1),
    ("w", 1, 0), ("o", 1, 2), ("ocy", 0, 0), ("ocy", 2, 0), ("ocy", 1, 0), ("w", 0, 2),
    ("ocy", 1, 2), ("ocy", 1, 1), ("ocy", 0, 1), ("owno", 3, 0), ("w", 1, 1), ("t", 0, 0),
    ("w", 1, 2), ("ocy", 2, 1), ("w", 0, 1), ("o", 0, 2), ("q1", 0, 0), ("w", 2, 0),
    ("kv1", 0, 0), ("w", 2, 1), ("w", 2, 2), ("o", 2, 2), ("ocy", 0, 2), ("ocx", 2, 0),
    ("kv2", 0, 0), ("o", 3, 2), ("q1", 1, 0), ("ocy", 2, 2), ("ocx", 2, 1), ("o", 3, 0),
    ("ocx", 0, 1), ("q2", 0, 0), ("ocx", 2, 2), ("ocx", 1, 2), ("ocx", 0, 2), ("ocx", 0, 0),
    ("att", 0, 0), ("ocx", 1, 0), ("ocx", 1, 1), ("o", 3, 1), ("q2", 1, 0), ("att", 1, 0),
    ("share", 0, 0), ("fin", 2, 0), ("fin", 1, 0), ("fin", 0, 0), ("fin", 3, 0),
)
ORDER_INNER = (
    ("owno", 0, 0), ("owno", 1, 0), ("owno", 2, 0), ("o", 0, 0), ("own", 0, 0), ("o", 1, 0),
    ("w", 0, 1), ("ocy", 0, 0), ("o", 2, 0), ("ocy", 1, 0), ("o", 1, 1), ("own", 1, 0),
    ("t", 0, 0), ("o", 0, 1), ("w", 1, 1), ("o", 1, 2), ("w", 0, 2), ("w", 1, 0), ("w", 2, 1),
    ("w", 1, 2), ("w", 0, 0), ("o", 0, 2), ("own", 2, 0), ("ocy", 1, 1), ("ocy", 2, 0),
    ("w", 2, 0), ("w", 2, 2), ("o", 2, 1), ("ocy", 1, 2), ("ocx", 0, 0), ("ocx", 0, 1),
    ("ocy", 0, 1), ("ocx", 2, 0), ("o", 3, 1), ("q1", 0, 0), ("o", 2, 2), ("ocx", 1, 2),
    ("ocx", 1, 0), ("kv1", 0, 0), ("ocx", 1, 1), ("o", 3, 2), ("owno", 3, 0), ("q1", 1, 0),
    ("ocx", 0, 2), ("ocy", 0, 2), ("kv2", 0, 0), ("o", 3, 0), ("q2", 0, 0), ("ocy", 2, 1),
    ("att", 0, 0), ("q2", 1, 0), ("att", 1, 0), ("ocx", 2, 1), ("share", 0, 0), ("ocx", 2, 2),
    ("ocy", 2, 2), ("fin", 1, 0), ("fin", 3, 0), ("fin", 0, 0), ("fin", 2, 0),
)


def pick(at, values):
    out = jnp.int32(values[0])
    for i, v in enumerate(values[1:]):
        out = jnp.where(at == i + 1, jnp.int32(v), out)
    return out


class Run:
    def __init__(self, ends):
        self.ends = ends
        self.sent = [0] * BULK

    def begin(self, c, kind, ref):
        c.start()
        self.sent[kind] += math.prod(ref.shape)


def kernel(
    n, chosen, live, tokens, query_w, key_w, value_w, out_w, listing, mixed,
    tok, other, weights, outs, lists, table, picked, mine_kv, mine_q, away, back,
    queries, bias, attended, local_sem, send_sem, recv_sem,
):
    dp, me, tp = lax.axis_index("dp"), lax.axis_index("kv"), lax.axis_index("tp")
    x_at, y_at = lax.rem(dp, 2), lax.div(dp, 2)
    right, left = jnp.minimum(me + 1, n - 1), jnp.maximum(me - 1, 0)
    to_x = {"dp": 2 * y_at + (1 - x_at)}
    to_y = {"dp": 2 * (1 - y_at) + x_at}
    dp_x, dp_y = 2 * y_at + (1 - x_at), 2 * (1 - y_at) + x_at
    dp_far = 2 * (1 - y_at) + (1 - x_at)
    side = lax.rem(x_at + y_at, 2)
    partner = {"tp": 1 - tp}
    rows = other.shape[0]
    depth = tok.shape[1]
    per_dev = rows // BLOCK
    seg = depth // n
    half_seg = seg // 2
    width = weights.shape[1]
    groups = weights.shape[0] // depth
    chunks = len(MODES)
    owned = outs.shape[0] // chunks // n
    tall = n * owned
    tile = outs.shape[1]
    is_end = jnp.logical_or(me == 0, me == n - 1)
    inward = {"kv": jnp.where(me == 0, right, left)}
    near = [pick(me, v) for v in ((1, 2, 1, 2), (2, 0, 3, 1), (3, 3, 0, 0))]

    def load(src, dst, at):
        c = pltpu.make_async_copy(src, dst, local_sem.at[at])
        c.start()

    def loaded(ref, at):
        pltpu.make_async_copy(ref, ref, local_sem.at[at]).wait()

    def remote(src, dst, send, recv, target):
        return pltpu.make_async_remote_copy(
            src_ref=src, dst_ref=dst, send_sem=send_sem.at[send], recv_sem=recv_sem.at[recv],
            device_id=target, device_id_type=MESH,
        )

    def arrived(ref, recv):
        remote(ref, ref, 0, recv, partner).wait_recv()

    my_rows = pl.ds(pl.multiple_of(x_at * seg, seg), seg)

    def slab(group):
        return pl.ds(pl.multiple_of(group * depth + me * seg, seg), seg)

    load(key_w.at[my_rows, :], weights.at[slab(0), :HD], 0)
    load(value_w.at[my_rows, :], weights.at[slab(0), HD:], 0)
    for i in range(groups - 1):
        load(query_w.at[my_rows, i * width : (i + 1) * width], weights.at[slab(1 + i), :], 0)
    for s in range(chunks):
        load(
            out_w.at[:, s * tile : (s + 1) * tile],
            outs.at[pl.ds(pl.multiple_of(s * tall + me * owned, owned), owned), :],
            1,
        )
    for k in range(n):
        load(
            tokens.at[:, pl.ds(pl.multiple_of((2 * k + x_at) * seg, seg), seg)],
            tok.at[:, k * seg : (k + 1) * seg],
            2,
        )
    load(listing, lists.at[me], 3)

    with jax.named_scope("barrier"):
        barrier = pltpu.get_barrier_semaphore()
        greeted = [{"kv": lax.rem(me + step, n)} for step in range(1, n)] + [to_x, to_y, partner]
        for target in greeted:
            pl.semaphore_signal(barrier, inc=1, device_id=target, device_id_type=MESH)
        pl.semaphore_wait(barrier, len(greeted))

    others = n - 1
    W = 0
    WY = W + groups * others
    O = WY + groups
    OX = O + chunks * others
    OY = OX + chunks * others
    OC = OY + chunks * others
    T = OC + chunks
    L = T + 2
    K = L + others
    Y = K + others
    S = Y + groups

    def from_owner(owner, receiver):
        return lax.rem(owner + n - receiver, n) - 1

    my_part = pl.ds(pl.multiple_of(tp * (rows // 2), rows // 2), rows // 2)
    their_part = pl.ds(pl.multiple_of((1 - tp) * (rows // 2), rows // 2), rows // 2)
    for k in range(n):
        cols = pl.ds(pl.multiple_of((2 * k + 1 - x_at) * seg, seg), seg)
        remote(
            tokens.at[my_part, cols], other.at[my_part, k * seg : (k + 1) * seg], BULK + 2 * others, T, to_x
        ).start()

    def t_share(run):
        piece = other.at[my_part, :]
        arrived(piece, T)
        run.begin(remote(piece, piece, REST, T + 1, partner), REST, piece)

    def l_copy(step):
        return remote(
            listing, lists.at[me], BULK + step - 1, L + step - 1, {"kv": jnp.maximum(me - step, 0)}
        )

    for step in range(1, n):
        pl.when(me >= step)(l_copy(step).start)

    def z_targets(run):
        return [inward] if run.ends else [{"kv": right}, {"kv": left}]

    def w_piece(group, owner, which):
        start = group * depth + owner * seg + which * half_seg
        return weights.at[pl.ds(pl.multiple_of(start, half_seg), half_seg), :]

    def w_own(run, group):
        piece = w_piece(group, me, y_at)
        for target in z_targets(run):
            recv = W + group * others + from_owner(me, target["kv"])
            run.begin(remote(piece, piece, WEIGHTS, recv, target), WEIGHTS, piece)

    def w_step(run, group, slot):
        owner = near[slot]
        piece = w_piece(group, owner, y_at)
        arrived(piece, W + group * others + from_owner(owner, me))
        if not run.ends:
            to = jnp.where(owner < me, right, left)
            recv = W + group * others + from_owner(owner, to)
            run.begin(remote(piece, piece, WEIGHTS, recv, {"kv": to}), WEIGHTS, piece)
        run.begin(remote(piece, piece, WEIGHTS, WY + group, to_y), WEIGHTS, piece)

    def w_arrive(group):
        arrived(weights.at[: others * half_seg, :], WY + group)

    quarter = owned // 4

    def o_piece(s, owner, first, size):
        start = s * tall + owner * owned + first
        return outs.at[pl.ds(pl.multiple_of(start, LEAST), size), :]

    def o_send(run, piece, recv, target):
        run.begin(remote(piece, piece, OUTS, recv, target), OUTS, piece)

    def carried(s, owner):
        if MODES[s] in CUTS:
            return o_piece(s, owner, dp * quarter, quarter)
        return o_piece(s, owner, side * 2 * quarter, 2 * quarter)

    def o_own(run, s):
        for target in z_targets(run):
            o_send(run, carried(s, me), O + s * others + from_owner(me, target["kv"]), target)

    def o_step(run, s, slot):
        owner = near[slot]
        piece = carried(s, owner)
        arrived(piece, O + s * others + from_owner(owner, me))
        if not run.ends:
            to = jnp.where(owner < me, right, left)
            o_send(run, piece, O + s * others + from_owner(owner, to), {"kv": to})
        if MODES[s] in CUTS:
            at = s * others + from_owner(owner, me)
            o_send(run, piece, OX + at, to_x)
            o_send(run, piece, OY + at, to_y)
        else:
            o_send(run, o_piece(s, owner, 2 * side * quarter, quarter), OC + s, to_x)
            o_send(run, o_piece(s, owner, (2 * side + 1) * quarter, quarter), OC + s, to_y)

    def o_turn(run, s, slot, along_x):
        owner, cut = near[slot], CUTS[MODES[s]]
        at = s * others + from_owner(owner, me)
        if along_x:
            arrived(o_piece(s, owner, dp_x * quarter, quarter), OX + at)
            o_send(run, o_piece(s, owner, dp_x * quarter, cut), OC + s, to_y)
        else:
            arrived(o_piece(s, owner, dp_y * quarter, quarter), OY + at)
            o_send(run, o_piece(s, owner, dp_y * quarter + cut, quarter - cut), OC + s, to_x)

    def o_arrive(s):
        count = 1 if MODES[s] in CUTS else 2
        arrived(outs.at[: others * count * quarter, :], OC + s)

    def part(source, group):
        return jnp.dot(
            source[...], weights[group * depth : (group + 1) * depth, :],
            preferred_element_type=jnp.float32,
        )

    def y_copy(group):
        return remote(away.at[group], back.at[group], REST, Y + group, to_x)

    def project(run, group):
        w_arrive(group)
        away[group] = part(other, group).astype(jnp.bfloat16)
        run.begin(y_copy(group), REST, away.at[group])
        if group == 0:
            mine_kv[...] = part(tok, group)
        else:
            mine_q[:, (group - 1) * width : group * width] = part(tok, group)

    slots = CAP * BLOCK
    local_at = n * slots

    def found(listed, block):
        return jnp.max((listed == block).astype(jnp.float32), axis=(0, 1), keepdims=True)

    def marks(listed, first):
        rank = jnp.zeros((1, 1), jnp.float32)
        out = [[] for _ in range(CAP)]
        for b in range(per_dev):
            one = found(listed, first + b)
            rank = rank + one
            for s in range(CAP):
                out[s].append(jnp.where(rank == s + 1, one, 0.0))
        return out

    def k_copy(step):
        return remote(
            picked.at[step - 1], table.at[pl.ds(pl.multiple_of(me * slots, slots), slots), :],
            BULK + others + step - 1, K + step - 1, {"kv": jnp.minimum(me + step, n - 1)},
        )

    def k_arrive():
        for step in range(1, n):
            pl.when(me >= step)(k_copy(step).wait_recv)

    def share_blocks(run):
        y_copy(0).wait_recv()
        full = (mine_kv[...] + back[0].astype(jnp.float32)).astype(jnp.bfloat16)
        table[local_at : local_at + rows, :] = full
        full = full.astype(jnp.float32)
        for step in range(1, n):
            pl.when(me + step < n)(l_copy(step).wait_recv)
        for step in range(1, n):

            def send_to(step=step):
                which = marks(lists[me + step], me * per_dev)
                for s in range(CAP):
                    kept = jnp.zeros((BLOCK, full.shape[1]), jnp.float32)
                    for b in range(per_dev):
                        kept = kept + which[s][b] * full[b * BLOCK : (b + 1) * BLOCK, :]
                    picked[step - 1, s * BLOCK : (s + 1) * BLOCK, :] = kept.astype(jnp.bfloat16)

            pl.when(me + step < n)(send_to)
            pl.when(me + step < n)(k_copy(step).start)

    def build_bias():
        loaded(lists.at[me], 3)
        listed = lists[me]
        seq = bias.shape[1]
        column = lax.broadcasted_iota(jnp.int32, (8, seq), 1)
        block = me * per_dev + lax.div(column - local_at, BLOCK)
        for owner in range(n):
            which = marks(listed, owner * per_dev)
            for s in range(CAP):
                ident = jnp.full((1, 1), -2.0, jnp.float32)
                for b in range(per_dev):
                    ident = jnp.where(which[s][b] > 0.5, float(owner * per_dev + b), ident)
                ident = jnp.where(me == owner, -2.0, ident).astype(jnp.int32)
                block = jnp.where(lax.div(column, BLOCK) == owner * CAP + s, ident, block)
        at = block * BLOCK + lax.rem(column, BLOCK)
        at = jnp.concatenate([at] * (BLOCK // 8), axis=0)
        row = lax.broadcasted_iota(jnp.int32, (BLOCK, seq), 0)
        for j in range(per_dev):
            open_to = jnp.full((8, seq), -jnp.inf, jnp.float32)
            for e in range(chosen.shape[1]):
                open_to = jnp.where(block == chosen[j, e], 0.0, open_to)
            spread = jnp.concatenate([open_to] * (BLOCK // 8), axis=0)
            causal = at <= row + (me * rows + j * BLOCK)
            bias[j * BLOCK : (j + 1) * BLOCK, :] = jnp.where(causal, spread, -jnp.inf)

    def queries_done(half):
        y_copy(1 + half).wait_recv()
        cols = slice(half * width, (half + 1) * width)
        queries[:, cols] = (
            mine_q[:, cols] + back[1 + half].astype(jnp.float32)
        ).astype(jnp.bfloat16)

    def attend(count, index):
        if index == 0:
            k_arrive()
        alive = me * rows + lax.broadcasted_iota(jnp.int32, (rows, HD), 0) < live[0]
        for h in range(count * index, count * (index + 1)):
            cols = slice(h * HD, (h + 1) * HD)
            scores = lax.dot_general(
                queries[:, cols], table[:, :HD], (((1,), (1,)), ((), ())),
                preferred_element_type=jnp.float32,
            )
            masked = scores * HD ** (-0.5) + bias[...]
            top = jnp.max(masked, axis=1, keepdims=True)
            probs = jnp.exp(masked - top)
            total = jnp.sum(probs, axis=1, keepdims=True)
            summed = jnp.dot(
                probs.astype(jnp.bfloat16), table[:, HD:], preferred_element_type=jnp.float32
            )
            attended[tp, :, cols] = jnp.where(alive, summed / total, 0.0).astype(jnp.bfloat16)

    def share(run):
        piece = attended.at[tp]
        run.begin(remote(piece, piece, REST, S, partner), REST, piece)
        arrived(attended.at[1 - tp], S)

    wide = queries.shape[1]

    def final(s):
        o_arrive(s)
        acc = jnp.dot(
            attended[0], outs[s * tall : s * tall + wide, :], preferred_element_type=jnp.float32
        )
        acc += jnp.dot(
            attended[1], outs[s * tall + wide : (s + 1) * tall, :],
            preferred_element_type=jnp.float32,
        )
        mixed[:, s * tile : (s + 1) * tile] = acc.astype(jnp.bfloat16)

    def settle():
        for owner in range(n):

            def clear(owner=owner):
                table[owner * slots : (owner + 1) * slots, :] = jnp.zeros(
                    (slots, table.shape[1]), table.dtype
                )

            pl.when(owner >= me)(clear)
        build_bias()
        loaded(tok, 2)

    def act(run, name, i, j):
        if name == "own":
            w_own(run, i)
        elif name == "owno":
            o_own(run, i)
        elif name == "t":
            t_share(run)
        elif name == "w":
            w_step(run, i, j)
        elif name == "o":
            o_step(run, i, j)
        elif name == "ocx" or name == "ocy":
            o_turn(run, i, j, name == "ocx")
        elif name == "kv1":
            project(run, 0)
        elif name == "kv2":
            share_blocks(run)
        elif name == "q1":
            project(run, 1 + i)
        elif name == "q2":
            queries_done(i)
        elif name == "att":
            attend(width // HD, i)
        elif name == "share":
            share(run)
        else:
            final(i)

    def follow(order, ends):
        run = Run(ends)
        begun = False
        projected = False
        for name, i, j in order:
            if not begun and not name.startswith("own"):
                settle()
                begun = True
            if not projected and name in ("kv1", "q1"):
                arrived(other.at[their_part, :], T + 1)
                projected = True
            with jax.named_scope(f"{name}_{i}_{j}"):
                act(run, name, i, j)
        with jax.named_scope("sent"):
            for kind, size in enumerate(run.sent):
                ref = outs.at[: size // tile, :]
                remote(ref, ref, kind, 0, partner).wait_send()

    loaded(weights.at[: groups * seg, :], 0)
    loaded(outs.at[: chunks * owned, :], 1)
    pl.when(is_end)(functools.partial(follow, ORDER_END, True))
    pl.when(jnp.logical_not(is_end))(functools.partial(follow, ORDER_INNER, False))
    ref = other.at[my_part, :]
    remote(ref, ref, BULK + 2 * others, T, to_x).wait_send()
    for step in range(1, n):
        pl.when(me >= step)(l_copy(step).wait_send)
        pl.when(me + step < n)(k_copy(step).wait_send)


def woven_body(tokens, query_weight, key_weight, value_weight, out_weight, chosen, live_length):
    n = lax.axis_size("kv")
    rows, model = tokens.shape
    wide = query_weight.shape[1]
    depth = model // HALF
    width = 2 * HD
    groups = 1 + wide // width
    chunks = len(MODES)
    tile = out_weight.shape[1] // chunks
    slots = CAP * BLOCK
    total = n * slots + rows
    dma = pltpu.SemaphoreType.DMA
    bf16 = jnp.bfloat16
    f32 = jnp.float32
    anywhere = pl.BlockSpec(memory_space=pl.ANY)
    small = pl.BlockSpec(memory_space=pltpu.SMEM)
    others = n - 1
    arrivals = groups * (others + 2) + chunks * (3 * others + 1) + 2 + 2 * others + 1
    return pl.pallas_call(
        functools.partial(kernel, n),
        out_shape=pltpu.VMEM((rows, out_weight.shape[1]), bf16),
        in_specs=[small, small] + [anywhere] * 6,
        out_specs=pl.BlockSpec(memory_space=pltpu.VMEM),
        scratch_shapes=[
            pltpu.VMEM((rows, depth), bf16),
            pltpu.VMEM((rows, depth), bf16),
            pltpu.VMEM((groups * depth, width), bf16),
            pltpu.VMEM((chunks * n * out_weight.shape[0], tile), bf16),
            pltpu.VMEM((n,) + chosen.shape, jnp.int32),
            pltpu.VMEM((total, width), bf16),
            pltpu.VMEM((n - 1, slots, width), bf16),
            pltpu.VMEM((rows, width), f32),
            pltpu.VMEM((rows, wide), f32),
            pltpu.VMEM((groups, rows, width), bf16),
            pltpu.VMEM((groups, rows, width), bf16),
            pltpu.VMEM((rows, wide), bf16),
            pltpu.VMEM((rows, total), f32),
            pltpu.VMEM((2, rows, wide), bf16),
            dma((4,)),
            dma((BULK + 2 * others + 1,)),
            dma((arrivals,)),
        ],
        compiler_params=pltpu.CompilerParams(
            collective_id=0, has_side_effects=True, vmem_limit_bytes=56 * 2**20
        ),
    )(chosen, live_length, tokens, query_weight, key_weight, value_weight, out_weight, chosen)


def solution(mesh):
    in_specs = (
        P(("dp", "kv"), None),
        P("kv", "tp"),
        P("kv", "tp"),
        P("kv", "tp"),
        P("kv", "tp"),
        P(("dp", "kv"), None),
        P("dp"),
    )
    out_specs = P(("dp", "kv"), "tp")
    fits = (mesh.shape["dp"], mesh.shape["kv"], mesh.shape["tp"]) == (4, 4, 2)
    body = woven_body if fits else gathered_body
    return jax.shard_map(body, mesh=mesh, in_specs=in_specs, out_specs=out_specs, check_vma=False)
```

time: 86.1 us -> 62.8 us (0.73)
  Pallas kernels: 77.5 us -> 60 us
  local copies, waits for them, and re-layouts: 7.59 us -> 0.97 us
    pallas_call x1, Pallas kernels: 77.5 us -> 60 us  [woven_body(): pl.pallas_call(functools.partial(kernel, n), out_shape=pltpu.VMEM((rows,...]
    unnamed x13 -> x1, local copies, waits for them, and re-layouts: 7.59 us -> 0.97 us
where the time goes in v2:
time: 62.8 us; the launch traced here: 61.6 us
  Pallas kernels  60 us (96%)
  local copies, waits for them, and re-layouts  0.97 us (2%)
  between operations  0.66 us (1%)
    pallas_call x1, Pallas kernels, woven_body(): pl.pallas_call(functools.partial(kernel, n), out_shape=pltpu.VMEM((rows,...  60 us

profile of v2, /device:TPU:0, one launch (start us, length us, event | category | flops | bytes accessed | tf_op | source)
XLA Modules:
  0.0 61.6 jit_solution(3514225197052940190)
XLA Ops:
  0.7 60.0 %shard_map.73 = bf16[256,2048]{1,0:T(8,128)(2,1)S(1)} custom-call(s32[8,16]{1,0:T(8,128)} %listing.1, s32[1]{0:T(128)S(6)} %copy.10.live, bf16[256,4096]{1,0:T(8,128)(2,1)} %tokens.1, bf16[1024,512]{1,0:T(8,128)(2,1)} %query_w.1, bf16[1024,128]{1,0:T(8,128)(2,1)} %key_w.1, bf16[1024,128]{1,0:T(8,128)(2,1)} %value_w.1, bf16[256,2048]{1,0:T(8,128)(2,1)} %out_w.1, ...), custom_call_target="tpu_custom_call" | custom-call | tf_op jit(solution)/shard_map/pallas_call | solution.py:553
  60.6 1.0 %copy.9 = bf16[256,2048]{1,0:T(8,128)(2,1)} copy(bf16[256,2048]{1,0:T(8,128)(2,1)S(1)} %shard_map.73) | data formatting | bytes 2097152

commit v3 on v2

--- a/solution.py
+++ b/solution.py
@@ -1,3 +1,4 @@
+import collections
 import functools
 import math
 
@@ -99,32 +100,47 @@
 HALF = 2
 LEAST = 16
 CUTS = {"q": 32, "p": 16}
-MODES = "ppph"
-WEIGHTS, OUTS, REST = range(3)
-BULK = 3
+MODES = "pppppphh"
+SHARES = (2, 2, 2, 2, 2, 2, 2, 2)
+HEADS = (2, 1, 1)
 ORDER_END = (
-    ("owno", 1, 0), ("own", 0, 0), ("owno", 0, 0), ("owno", 2, 0), ("own", 1, 0), ("o", 0, 0),
-    ("own", 2, 0), ("o", 1, 0), ("o", 2, 0), ("o", 0, 1), ("w", 0, 0), ("o", 2, 1), ("o", 1, 1),
-    ("w", 1, 0), ("o", 1, 2), ("ocy", 0, 0), ("ocy", 2, 0), ("ocy", 1, 0), ("w", 0, 2),
-    ("ocy", 1, 2), ("ocy", 1, 1), ("ocy", 0, 1), ("owno", 3, 0), ("w", 1, 1), ("t", 0, 0),
-    ("w", 1, 2), ("ocy", 2, 1), ("w", 0, 1), ("o", 0, 2), ("q1", 0, 0), ("w", 2, 0),
-    ("kv1", 0, 0), ("w", 2, 1), ("w", 2, 2), ("o", 2, 2), ("ocy", 0, 2), ("ocx", 2, 0),
-    ("kv2", 0, 0), ("o", 3, 2), ("q1", 1, 0), ("ocy", 2, 2), ("ocx", 2, 1), ("o", 3, 0),
-    ("ocx", 0, 1), ("q2", 0, 0), ("ocx", 2, 2), ("ocx", 1, 2), ("ocx", 0, 2), ("ocx", 0, 0),
-    ("att", 0, 0), ("ocx", 1, 0), ("ocx", 1, 1), ("o", 3, 1), ("q2", 1, 0), ("att", 1, 0),
-    ("share", 0, 0), ("fin", 2, 0), ("fin", 1, 0), ("fin", 0, 0), ("fin", 3, 0),
+    ("own", 0, 0), ("owno", 0, 0), ("owno", 4, 0), ("o", 2, 0), ("owno", 7, 0), ("o", 3, 0),
+    ("own", 2, 0), ("own", 3, 0), ("owno", 6, 0), ("owno", 2, 0), ("w", 0, 0), ("o", 0, 0),
+    ("ocy", 2, 0), ("owno", 5, 0), ("own", 1, 0), ("o", 2, 1), ("o", 5, 0), ("o", 3, 1),
+    ("w", 1, 0), ("t", 0, 0), ("w", 0, 1), ("ocy", 5, 0), ("ocy", 0, 0), ("owno", 3, 0),
+    ("ocy", 3, 1), ("w", 0, 2), ("o", 4, 0), ("o", 0, 1), ("o", 5, 1), ("o", 4, 2), ("ocy", 3, 0),
+    ("o", 1, 0), ("owno", 1, 0), ("o", 1, 1), ("o", 4, 1), ("o", 5, 2), ("w", 1, 1),
+    ("ocy", 1, 1), ("ocy", 2, 1), ("kv1", 0, 0), ("ocy", 5, 1), ("w", 1, 2), ("o", 0, 2),
+    ("ocy", 4, 1), ("ocy", 4, 0), ("w", 3, 0), ("ocy", 4, 2), ("ocx", 5, 1), ("w", 3, 2),
+    ("ocy", 0, 1), ("q1", 0, 0), ("ocy", 5, 2), ("ocx", 3, 0), ("w", 3, 1), ("w", 2, 0),
+    ("ocx", 2, 1), ("ocx", 5, 0), ("ocy", 0, 2), ("w", 2, 1), ("kv2", 0, 0), ("w", 2, 2),
+    ("ocy", 1, 0), ("o", 3, 2), ("ocx", 0, 2), ("ocx", 3, 1), ("o", 1, 2), ("ocx", 4, 0),
+    ("q1", 2, 0), ("o", 7, 0), ("ocx", 1, 1), ("ocx", 5, 2), ("ocx", 4, 2), ("ocx", 4, 1),
+    ("ocx", 1, 0), ("o", 2, 2), ("o", 6, 0), ("q1", 1, 0), ("ocy", 3, 2), ("q2", 2, 0),
+    ("q2", 0, 0), ("ocx", 2, 0), ("ocx", 2, 2), ("ocx", 1, 2), ("ocx", 0, 1), ("ocx", 3, 2),
+    ("ocy", 1, 2), ("o", 6, 2), ("att", 0, 0), ("o", 6, 1), ("q2", 1, 0), ("ocx", 0, 0),
+    ("ocy", 2, 2), ("o", 7, 2), ("att", 1, 0), ("att", 2, 0), ("share", 0, 0), ("o", 7, 1),
+    ("fin", 5, 0), ("fin", 4, 0), ("fin", 0, 0), ("fin", 3, 0), ("fin", 6, 0), ("fin", 2, 0),
+    ("fin", 1, 0), ("fin", 7, 0),
 )
 ORDER_INNER = (
-    ("owno", 0, 0), ("owno", 1, 0), ("owno", 2, 0), ("o", 0, 0), ("own", 0, 0), ("o", 1, 0),
-    ("w", 0, 1), ("ocy", 0, 0), ("o", 2, 0), ("ocy", 1, 0), ("o", 1, 1), ("own", 1, 0),
-    ("t", 0, 0), ("o", 0, 1), ("w", 1, 1), ("o", 1, 2), ("w", 0, 2), ("w", 1, 0), ("w", 2, 1),
-    ("w", 1, 2), ("w", 0, 0), ("o", 0, 2), ("own", 2, 0), ("ocy", 1, 1), ("ocy", 2, 0),
-    ("w", 2, 0), ("w", 2, 2), ("o", 2, 1), ("ocy", 1, 2), ("ocx", 0, 0), ("ocx", 0, 1),
-    ("ocy", 0, 1), ("ocx", 2, 0), ("o", 3, 1), ("q1", 0, 0), ("o", 2, 2), ("ocx", 1, 2),
-    ("ocx", 1, 0), ("kv1", 0, 0), ("ocx", 1, 1), ("o", 3, 2), ("owno", 3, 0), ("q1", 1, 0),
-    ("ocx", 0, 2), ("ocy", 0, 2), ("kv2", 0, 0), ("o", 3, 0), ("q2", 0, 0), ("ocy", 2, 1),
-    ("att", 0, 0), ("q2", 1, 0), ("att", 1, 0), ("ocx", 2, 1), ("share", 0, 0), ("ocx", 2, 2),
-    ("ocy", 2, 2), ("fin", 1, 0), ("fin", 3, 0), ("fin", 0, 0), ("fin", 2, 0),
+    ("owno", 3, 0), ("owno", 2, 0), ("own", 0, 0), ("owno", 0, 0), ("o", 3, 0), ("o", 2, 0),
+    ("w", 0, 1), ("owno", 5, 0), ("own", 1, 0), ("w", 0, 0), ("w", 0, 2), ("owno", 4, 0),
+    ("o", 0, 0), ("owno", 1, 0), ("o", 4, 1), ("o", 0, 1), ("o", 5, 1), ("o", 1, 0), ("o", 4, 2),
+    ("o", 5, 0), ("w", 3, 1), ("w", 1, 1), ("o", 4, 0), ("t", 0, 0), ("o", 3, 1), ("o", 5, 2),
+    ("ocy", 5, 1), ("kv1", 0, 0), ("w", 1, 0), ("ocy", 0, 0), ("ocx", 1, 0), ("w", 1, 2),
+    ("ocy", 1, 0), ("own", 2, 0), ("o", 0, 2), ("own", 3, 0), ("ocy", 4, 0), ("w", 3, 2),
+    ("ocy", 2, 0), ("w", 2, 1), ("w", 3, 0), ("o", 3, 2), ("w", 2, 0), ("ocx", 0, 2), ("o", 1, 1),
+    ("ocy", 5, 2), ("w", 2, 2), ("ocy", 3, 1), ("o", 1, 2), ("ocy", 4, 2), ("ocx", 4, 0),
+    ("owno", 6, 0), ("ocy", 3, 0), ("ocy", 0, 1), ("owno", 7, 0), ("ocx", 0, 0), ("o", 6, 1),
+    ("ocx", 0, 1), ("q1", 0, 0), ("ocx", 1, 2), ("o", 2, 1), ("o", 2, 2), ("q1", 2, 0),
+    ("ocx", 4, 1), ("o", 7, 1), ("ocx", 2, 0), ("ocy", 4, 1), ("kv2", 0, 0), ("ocx", 5, 1),
+    ("o", 6, 2), ("q2", 0, 0), ("ocy", 5, 0), ("ocx", 3, 2), ("o", 6, 0), ("q1", 1, 0),
+    ("ocy", 1, 2), ("o", 7, 2), ("o", 7, 0), ("ocx", 5, 2), ("ocy", 0, 2), ("att", 0, 0),
+    ("q2", 1, 0), ("ocy", 3, 2), ("ocx", 2, 1), ("ocx", 1, 1), ("ocy", 1, 1), ("ocx", 5, 0),
+    ("ocx", 3, 0), ("q2", 2, 0), ("ocx", 4, 2), ("att", 1, 0), ("att", 2, 0), ("ocy", 2, 2),
+    ("ocx", 3, 1), ("ocx", 2, 2), ("share", 0, 0), ("ocy", 2, 1), ("fin", 0, 0), ("fin", 6, 0),
+    ("fin", 1, 0), ("fin", 7, 0), ("fin", 5, 0), ("fin", 3, 0), ("fin", 4, 0), ("fin", 2, 0),
 )
 
 
@@ -138,7 +154,7 @@
 class Run:
     def __init__(self, ends):
         self.ends = ends
-        self.sent = [0] * BULK
+        self.sent = collections.defaultdict(int)
 
     def begin(self, c, kind, ref):
         c.start()
@@ -146,9 +162,9 @@
 
 
 def kernel(
-    n, chosen, live, tokens, query_w, key_w, value_w, out_w, listing, mixed,
+    n, tokens, query_w, key_w, value_w, out_w, listing, live_in, mixed,
     tok, other, weights, outs, lists, table, picked, mine_kv, mine_q, away, back,
-    queries, bias, attended, local_sem, send_sem, recv_sem,
+    queries, bias, attended, chosen, live, local_sem, send_sem, recv_sem,
 ):
     dp, me, tp = lax.axis_index("dp"), lax.axis_index("kv"), lax.axis_index("tp")
     x_at, y_at = lax.rem(dp, 2), lax.div(dp, 2)
@@ -164,12 +180,11 @@
     per_dev = rows // BLOCK
     seg = depth // n
     half_seg = seg // 2
-    width = weights.shape[1]
-    groups = weights.shape[0] // depth
-    chunks = len(MODES)
-    owned = outs.shape[0] // chunks // n
-    tall = n * owned
-    tile = outs.shape[1]
+    groups, chunks = len(weights), len(outs)
+    widths = [ref.shape[1] for ref in weights]
+    firsts = [sum(widths[1:g]) for g in range(groups)]
+    tiles = [ref.shape[1] for ref in outs]
+    owned = outs[0].shape[0] // n
     is_end = jnp.logical_or(me == 0, me == n - 1)
     inward = {"kv": jnp.where(me == 0, right, left)}
     near = [pick(me, v) for v in ((1, 2, 1, 2), (2, 0, 3, 1), (3, 3, 0, 0))]
@@ -190,34 +205,36 @@
     def arrived(ref, recv):
         remote(ref, ref, 0, recv, partner).wait_recv()
 
+    barrier = pltpu.get_barrier_semaphore()
+    greeted = [{"kv": lax.rem(me + step, n)} for step in range(1, n)] + [to_x, to_y, partner]
+    for target in greeted:
+        pl.semaphore_signal(barrier, inc=1, device_id=target, device_id_type=MESH)
+
     my_rows = pl.ds(pl.multiple_of(x_at * seg, seg), seg)
-
-    def slab(group):
-        return pl.ds(pl.multiple_of(group * depth + me * seg, seg), seg)
-
-    load(key_w.at[my_rows, :], weights.at[slab(0), :HD], 0)
-    load(value_w.at[my_rows, :], weights.at[slab(0), HD:], 0)
-    for i in range(groups - 1):
-        load(query_w.at[my_rows, i * width : (i + 1) * width], weights.at[slab(1 + i), :], 0)
+    my_slab = pl.ds(pl.multiple_of(me * seg, seg), seg)
     for s in range(chunks):
         load(
-            out_w.at[:, s * tile : (s + 1) * tile],
-            outs.at[pl.ds(pl.multiple_of(s * tall + me * owned, owned), owned), :],
-            1,
-        )
+            out_w.at[:, sum(tiles[:s]) : sum(tiles[: s + 1])],
+            outs[s].at[pl.ds(pl.multiple_of(me * owned, owned), owned), :],
+            groups + s,
+        )
+    load(key_w.at[my_rows, :], weights[0].at[my_slab, :HD], 0)
+    load(value_w.at[my_rows, :], weights[0].at[my_slab, HD:], 0)
+    for g in range(1, groups):
+        load(
+            query_w.at[my_rows, firsts[g] : firsts[g] + widths[g]], weights[g].at[my_slab, :], g
+        )
+    load(listing, lists.at[me], groups + chunks)
+    load(listing, chosen, groups + chunks + 1)
+    load(live_in, live, groups + chunks + 2)
     for k in range(n):
         load(
             tokens.at[:, pl.ds(pl.multiple_of((2 * k + x_at) * seg, seg), seg)],
             tok.at[:, k * seg : (k + 1) * seg],
-            2,
-        )
-    load(listing, lists.at[me], 3)
+            groups + chunks + 3,
+        )
 
     with jax.named_scope("barrier"):
-        barrier = pltpu.get_barrier_semaphore()
-        greeted = [{"kv": lax.rem(me + step, n)} for step in range(1, n)] + [to_x, to_y, partner]
-        for target in greeted:
-            pl.semaphore_signal(barrier, inc=1, device_id=target, device_id_type=MESH)
         pl.semaphore_wait(barrier, len(greeted))
 
     others = n - 1
@@ -232,6 +249,9 @@
     K = L + others
     Y = K + others
     S = Y + groups
+    REST = groups + chunks
+    FORTH, TOKENS, LISTS = REST + 1, REST + 2, REST + 3
+    BLOCKS = LISTS + others
 
     def from_owner(owner, receiver):
         return lax.rem(owner + n - receiver, n) - 1
@@ -241,17 +261,17 @@
     for k in range(n):
         cols = pl.ds(pl.multiple_of((2 * k + 1 - x_at) * seg, seg), seg)
         remote(
-            tokens.at[my_part, cols], other.at[my_part, k * seg : (k + 1) * seg], BULK + 2 * others, T, to_x
+            tokens.at[my_part, cols], other.at[my_part, k * seg : (k + 1) * seg], TOKENS, T, to_x
         ).start()
 
     def t_share(run):
         piece = other.at[my_part, :]
         arrived(piece, T)
-        run.begin(remote(piece, piece, REST, T + 1, partner), REST, piece)
+        run.begin(remote(piece, piece, FORTH, T + 1, partner), FORTH, piece)
 
     def l_copy(step):
         return remote(
-            listing, lists.at[me], BULK + step - 1, L + step - 1, {"kv": jnp.maximum(me - step, 0)}
+            listing, lists.at[me], LISTS + step - 1, L + step - 1, {"kv": jnp.maximum(me - step, 0)}
         )
 
     for step in range(1, n):
@@ -261,14 +281,15 @@
         return [inward] if run.ends else [{"kv": right}, {"kv": left}]
 
     def w_piece(group, owner, which):
-        start = group * depth + owner * seg + which * half_seg
-        return weights.at[pl.ds(pl.multiple_of(start, half_seg), half_seg), :]
+        start = owner * seg + which * half_seg
+        return weights[group].at[pl.ds(pl.multiple_of(start, half_seg), half_seg), :]
 
     def w_own(run, group):
+        loaded(weights[group].at[:seg, :], group)
         piece = w_piece(group, me, y_at)
         for target in z_targets(run):
             recv = W + group * others + from_owner(me, target["kv"])
-            run.begin(remote(piece, piece, WEIGHTS, recv, target), WEIGHTS, piece)
+            run.begin(remote(piece, piece, group, recv, target), group, piece)
 
     def w_step(run, group, slot):
         owner = near[slot]
@@ -277,20 +298,20 @@
         if not run.ends:
             to = jnp.where(owner < me, right, left)
             recv = W + group * others + from_owner(owner, to)
-            run.begin(remote(piece, piece, WEIGHTS, recv, {"kv": to}), WEIGHTS, piece)
-        run.begin(remote(piece, piece, WEIGHTS, WY + group, to_y), WEIGHTS, piece)
+            run.begin(remote(piece, piece, group, recv, {"kv": to}), group, piece)
+        run.begin(remote(piece, piece, group, WY + group, to_y), group, piece)
 
     def w_arrive(group):
-        arrived(weights.at[: others * half_seg, :], WY + group)
+        arrived(weights[group].at[: others * half_seg, :], WY + group)
 
     quarter = owned // 4
 
     def o_piece(s, owner, first, size):
-        start = s * tall + owner * owned + first
-        return outs.at[pl.ds(pl.multiple_of(start, LEAST), size), :]
-
-    def o_send(run, piece, recv, target):
-        run.begin(remote(piece, piece, OUTS, recv, target), OUTS, piece)
+        return outs[s].at[pl.ds(pl.multiple_of(owner * owned + first, LEAST), size), :]
+
+    def o_send(run, s, piece, recv, target):
+        kind = groups + s
+        run.begin(remote(piece, piece, kind, recv, target), kind, piece)
 
     def carried(s, owner):
         if MODES[s] in CUTS:
@@ -298,8 +319,9 @@
         return o_piece(s, owner, side * 2 * quarter, 2 * quarter)
 
     def o_own(run, s):
+        loaded(outs[s].at[:owned, :], groups + s)
         for target in z_targets(run):
-            o_send(run, carried(s, me), O + s * others + from_owner(me, target["kv"]), target)
+            o_send(run, s, carried(s, me), O + s * others + from_owner(me, target["kv"]), target)
 
     def o_step(run, s, slot):
         owner = near[slot]
@@ -307,46 +329,45 @@
         arrived(piece, O + s * others + from_owner(owner, me))
         if not run.ends:
             to = jnp.where(owner < me, right, left)
-            o_send(run, piece, O + s * others + from_owner(owner, to), {"kv": to})
+            o_send(run, s, piece, O + s * others + from_owner(owner, to), {"kv": to})
         if MODES[s] in CUTS:
             at = s * others + from_owner(owner, me)
-            o_send(run, piece, OX + at, to_x)
-            o_send(run, piece, OY + at, to_y)
+            o_send(run, s, piece, OX + at, to_x)
+            o_send(run, s, piece, OY + at, to_y)
         else:
-            o_send(run, o_piece(s, owner, 2 * side * quarter, quarter), OC + s, to_x)
-            o_send(run, o_piece(s, owner, (2 * side + 1) * quarter, quarter), OC + s, to_y)
+            o_send(run, s, o_piece(s, owner, 2 * side * quarter, quarter), OC + s, to_x)
+            o_send(run, s, o_piece(s, owner, (2 * side + 1) * quarter, quarter), OC + s, to_y)
 
     def o_turn(run, s, slot, along_x):
         owner, cut = near[slot], CUTS[MODES[s]]
         at = s * others + from_owner(owner, me)
         if along_x:
             arrived(o_piece(s, owner, dp_x * quarter, quarter), OX + at)
-            o_send(run, o_piece(s, owner, dp_x * quarter, cut), OC + s, to_y)
+            o_send(run, s, o_piece(s, owner, dp_x * quarter, cut), OC + s, to_y)
         else:
             arrived(o_piece(s, owner, dp_y * quarter, quarter), OY + at)
-            o_send(run, o_piece(s, owner, dp_y * quarter + cut, quarter - cut), OC + s, to_x)
+            o_send(run, s, o_piece(s, owner, dp_y * quarter + cut, quarter - cut), OC + s, to_x)
 
     def o_arrive(s):
         count = 1 if MODES[s] in CUTS else 2
-        arrived(outs.at[: others * count * quarter, :], OC + s)
+        arrived(outs[s].at[: others * count * quarter, :], OC + s)
 
     def part(source, group):
         return jnp.dot(
-            source[...], weights[group * depth : (group + 1) * depth, :],
-            preferred_element_type=jnp.float32,
+            source[...], weights[group][...], preferred_element_type=jnp.float32
         )
 
     def y_copy(group):
-        return remote(away.at[group], back.at[group], REST, Y + group, to_x)
+        return remote(away[group], back[group], REST, Y + group, to_x)
 
     def project(run, group):
         w_arrive(group)
-        away[group] = part(other, group).astype(jnp.bfloat16)
-        run.begin(y_copy(group), REST, away.at[group])
+        away[group][...] = part(other, group).astype(jnp.bfloat16)
+        run.begin(y_copy(group), REST, away[group])
         if group == 0:
             mine_kv[...] = part(tok, group)
         else:
-            mine_q[:, (group - 1) * width : group * width] = part(tok, group)
+            mine_q[:, firsts[group] : firsts[group] + widths[group]] = part(tok, group)
 
     slots = CAP * BLOCK
     local_at = n * slots
@@ -367,7 +388,7 @@
     def k_copy(step):
         return remote(
             picked.at[step - 1], table.at[pl.ds(pl.multiple_of(me * slots, slots), slots), :],
-            BULK + others + step - 1, K + step - 1, {"kv": jnp.minimum(me + step, n - 1)},
+            BLOCKS + step - 1, K + step - 1, {"kv": jnp.minimum(me + step, n - 1)},
         )
 
     def k_arrive():
@@ -376,7 +397,7 @@
 
     def share_blocks(run):
         y_copy(0).wait_recv()
-        full = (mine_kv[...] + back[0].astype(jnp.float32)).astype(jnp.bfloat16)
+        full = (mine_kv[...] + back[0][...].astype(jnp.float32)).astype(jnp.bfloat16)
         table[local_at : local_at + rows, :] = full
         full = full.astype(jnp.float32)
         for step in range(1, n):
@@ -395,7 +416,9 @@
             pl.when(me + step < n)(k_copy(step).start)
 
     def build_bias():
-        loaded(lists.at[me], 3)
+        loaded(lists.at[me], groups + chunks)
+        loaded(chosen, groups + chunks + 1)
+        loaded(live, groups + chunks + 2)
         listed = lists[me]
         seq = bias.shape[1]
         column = lax.broadcasted_iota(jnp.int32, (8, seq), 1)
@@ -419,18 +442,18 @@
             causal = at <= row + (me * rows + j * BLOCK)
             bias[j * BLOCK : (j + 1) * BLOCK, :] = jnp.where(causal, spread, -jnp.inf)
 
-    def queries_done(half):
-        y_copy(1 + half).wait_recv()
-        cols = slice(half * width, (half + 1) * width)
+    def queries_done(group):
+        y_copy(group).wait_recv()
+        cols = slice(firsts[group], firsts[group] + widths[group])
         queries[:, cols] = (
-            mine_q[:, cols] + back[1 + half].astype(jnp.float32)
+            mine_q[:, cols] + back[group][...].astype(jnp.float32)
         ).astype(jnp.bfloat16)
 
-    def attend(count, index):
-        if index == 0:
+    def attend(group):
+        if group == 1:
             k_arrive()
         alive = me * rows + lax.broadcasted_iota(jnp.int32, (rows, HD), 0) < live[0]
-        for h in range(count * index, count * (index + 1)):
+        for h in range(firsts[group] // HD, (firsts[group] + widths[group]) // HD):
             cols = slice(h * HD, (h + 1) * HD)
             scores = lax.dot_general(
                 queries[:, cols], table[:, :HD], (((1,), (1,)), ((), ())),
@@ -455,13 +478,12 @@
     def final(s):
         o_arrive(s)
         acc = jnp.dot(
-            attended[0], outs[s * tall : s * tall + wide, :], preferred_element_type=jnp.float32
+            attended[0], outs[s][:wide, :], preferred_element_type=jnp.float32
         )
         acc += jnp.dot(
-            attended[1], outs[s * tall + wide : (s + 1) * tall, :],
-            preferred_element_type=jnp.float32,
-        )
-        mixed[:, s * tile : (s + 1) * tile] = acc.astype(jnp.bfloat16)
+            attended[1], outs[s][wide:, :], preferred_element_type=jnp.float32
+        )
+        mixed[:, sum(tiles[:s]) : sum(tiles[: s + 1])] = acc.astype(jnp.bfloat16)
 
     def settle():
         for owner in range(n):
@@ -473,7 +495,7 @@
 
             pl.when(owner >= me)(clear)
         build_bias()
-        loaded(tok, 2)
+        loaded(tok, groups + chunks + 3)
 
     def act(run, name, i, j):
         if name == "own":
@@ -495,9 +517,9 @@
         elif name == "q1":
             project(run, 1 + i)
         elif name == "q2":
-            queries_done(i)
+            queries_done(1 + i)
         elif name == "att":
-            attend(width // HD, i)
+            attend(1 + i)
         elif name == "share":
             share(run)
         else:
@@ -516,17 +538,19 @@
                 projected = True
             with jax.named_scope(f"{name}_{i}_{j}"):
                 act(run, name, i, j)
-        with jax.named_scope("sent"):
-            for kind, size in enumerate(run.sent):
-                ref = outs.at[: size // tile, :]
-                remote(ref, ref, kind, 0, partner).wait_send()
-
-    loaded(weights.at[: groups * seg, :], 0)
-    loaded(outs.at[: chunks * owned, :], 1)
+        for kind, size in run.sent.items():
+            if kind < groups:
+                ref = weights[kind].at[: size // widths[kind], :]
+            elif kind < groups + chunks:
+                ref = outs[kind - groups].at[: size // tiles[kind - groups], :]
+            else:
+                ref = tok.at[:, : size // rows]
+            remote(ref, ref, kind, 0, partner).wait_send()
+
     pl.when(is_end)(functools.partial(follow, ORDER_END, True))
     pl.when(jnp.logical_not(is_end))(functools.partial(follow, ORDER_INNER, False))
     ref = other.at[my_part, :]
-    remote(ref, ref, BULK + 2 * others, T, to_x).wait_send()
+    remote(ref, ref, TOKENS, T, to_x).wait_send()
     for step in range(1, n):
         pl.when(me >= step)(l_copy(step).wait_send)
         pl.when(me + step < n)(k_copy(step).wait_send)
@@ -538,46 +562,48 @@
     wide = query_weight.shape[1]
     depth = model // HALF
     width = 2 * HD
-    groups = 1 + wide // width
-    chunks = len(MODES)
-    tile = out_weight.shape[1] // chunks
+    widths = [width] + [heads * HD for heads in HEADS]
+    unit = out_weight.shape[1] // sum(SHARES)
+    tiles = [share * unit for share in SHARES]
+    groups, chunks = len(widths), len(tiles)
     slots = CAP * BLOCK
     total = n * slots + rows
     dma = pltpu.SemaphoreType.DMA
     bf16 = jnp.bfloat16
     f32 = jnp.float32
     anywhere = pl.BlockSpec(memory_space=pl.ANY)
-    small = pl.BlockSpec(memory_space=pltpu.SMEM)
     others = n - 1
     arrivals = groups * (others + 2) + chunks * (3 * others + 1) + 2 + 2 * others + 1
     return pl.pallas_call(
         functools.partial(kernel, n),
         out_shape=pltpu.VMEM((rows, out_weight.shape[1]), bf16),
-        in_specs=[small, small] + [anywhere] * 6,
+        in_specs=[anywhere] * 7,
         out_specs=pl.BlockSpec(memory_space=pltpu.VMEM),
         scratch_shapes=[
             pltpu.VMEM((rows, depth), bf16),
             pltpu.VMEM((rows, depth), bf16),
-            pltpu.VMEM((groups * depth, width), bf16),
-            pltpu.VMEM((chunks * n * out_weight.shape[0], tile), bf16),
+            tuple(pltpu.VMEM((depth, w), bf16) for w in widths),
+            tuple(pltpu.VMEM((n * out_weight.shape[0], w), bf16) for w in tiles),
             pltpu.VMEM((n,) + chosen.shape, jnp.int32),
             pltpu.VMEM((total, width), bf16),
             pltpu.VMEM((n - 1, slots, width), bf16),
             pltpu.VMEM((rows, width), f32),
             pltpu.VMEM((rows, wide), f32),
-            pltpu.VMEM((groups, rows, width), bf16),
-            pltpu.VMEM((groups, rows, width), bf16),
+            tuple(pltpu.VMEM((rows, w), bf16) for w in widths),
+            tuple(pltpu.VMEM((rows, w), bf16) for w in widths),
             pltpu.VMEM((rows, wide), bf16),
             pltpu.VMEM((rows, total), f32),
             pltpu.VMEM((2, rows, wide), bf16),
-            dma((4,)),
-            dma((BULK + 2 * others + 1,)),
+            pltpu.SMEM(chosen.shape, jnp.int32),
+            pltpu.SMEM(live_length.shape, jnp.int32),
+            dma((groups + chunks + 4,)),
+            dma((groups + chunks + 3 + 2 * others,)),
             dma((arrivals,)),
         ],
         compiler_params=pltpu.CompilerParams(
             collective_id=0, has_side_effects=True, vmem_limit_bytes=56 * 2**20
         ),
-    )(chosen, live_length, tokens, query_weight, key_weight, value_weight, out_weight, chosen)
+    )(tokens, query_weight, key_weight, value_weight, out_weight, chosen, live_length)
 
 
 def solution(mesh):

time: 62.8 us -> 63.3 us (level); the launches traced: 61.6 us -> 63.2 us
  Pallas kernels: 60 us -> 61.5 us
    pallas_call x1, Pallas kernels: 60 us -> 61.5 us  [woven_body(): pl.pallas_call(functools.partial(kernel, n), out_shape=pltpu.VMEM((rows,...]
where the time goes in v3:
time: 63.3 us; the launch traced here: 63.2 us
  Pallas kernels  61.5 us (97%)
  local copies, waits for them, and re-layouts  0.97 us (2%)
  between operations  0.66 us (1%)
    pallas_call x1, Pallas kernels, woven_body(): pl.pallas_call(functools.partial(kernel, n), out_shape=pltpu.VMEM((rows,...  61.5 us

profile of v3, /device:TPU:0, one launch (start us, length us, event | category | flops | bytes accessed | tf_op | source)
XLA Modules:
  0.0 63.2 jit_solution(3477218181879467302)
XLA Ops:
  0.7 61.5 %shard_map.73 = bf16[256,2048]{1,0:T(8,128)(2,1)S(1)} custom-call(bf16[256,4096]{1,0:T(8,128)(2,1)} %tokens.1, bf16[1024,512]{1,0:T(8,128)(2,1)} %query_w.1, bf16[1024,128]{1,0:T(8,128)(2,1)} %key_w.1, bf16[1024,128]{1,0:T(8,128)(2,1)} %value_w.1, bf16[256,2048]{1,0:T(8,128)(2,1)} %out_w.1, s32[8,16]{1,0:T(8,128)} %listing.1, s32[1]{0:T(128)S(6)} %copy.10.live_in), custom_call_target="tpu_custom_call" | custom-call | tf_op jit(solution)/shard_map/pallas_call | solution.py:577
  62.2 1.0 %copy.9 = bf16[256,2048]{1,0:T(8,128)(2,1)} copy(bf16[256,2048]{1,0:T(8,128)(2,1)S(1)} %shard_map.73) | data formatting | bytes 2097152

commit v4 on v3

--- a/solution.py
+++ b/solution.py
@@ -100,47 +100,34 @@
 HALF = 2
 LEAST = 16
 CUTS = {"q": 32, "p": 16}
-MODES = "pppppphh"
-SHARES = (2, 2, 2, 2, 2, 2, 2, 2)
-HEADS = (2, 1, 1)
+MODES = "ppph"
+SHARES = (4, 4, 4, 4)
+HEADS = (2, 2)
 ORDER_END = (
-    ("own", 0, 0), ("owno", 0, 0), ("owno", 4, 0), ("o", 2, 0), ("owno", 7, 0), ("o", 3, 0),
-    ("own", 2, 0), ("own", 3, 0), ("owno", 6, 0), ("owno", 2, 0), ("w", 0, 0), ("o", 0, 0),
-    ("ocy", 2, 0), ("owno", 5, 0), ("own", 1, 0), ("o", 2, 1), ("o", 5, 0), ("o", 3, 1),
-    ("w", 1, 0), ("t", 0, 0), ("w", 0, 1), ("ocy", 5, 0), ("ocy", 0, 0), ("owno", 3, 0),
-    ("ocy", 3, 1), ("w", 0, 2), ("o", 4, 0), ("o", 0, 1), ("o", 5, 1), ("o", 4, 2), ("ocy", 3, 0),
-    ("o", 1, 0), ("owno", 1, 0), ("o", 1, 1), ("o", 4, 1), ("o", 5, 2), ("w", 1, 1),
-    ("ocy", 1, 1), ("ocy", 2, 1), ("kv1", 0, 0), ("ocy", 5, 1), ("w", 1, 2), ("o", 0, 2),
-    ("ocy", 4, 1), ("ocy", 4, 0), ("w", 3, 0), ("ocy", 4, 2), ("ocx", 5, 1), ("w", 3, 2),
-    ("ocy", 0, 1), ("q1", 0, 0), ("ocy", 5, 2), ("ocx", 3, 0), ("w", 3, 1), ("w", 2, 0),
-    ("ocx", 2, 1), ("ocx", 5, 0), ("ocy", 0, 2), ("w", 2, 1), ("kv2", 0, 0), ("w", 2, 2),
-    ("ocy", 1, 0), ("o", 3, 2), ("ocx", 0, 2), ("ocx", 3, 1), ("o", 1, 2), ("ocx", 4, 0),
-    ("q1", 2, 0), ("o", 7, 0), ("ocx", 1, 1), ("ocx", 5, 2), ("ocx", 4, 2), ("ocx", 4, 1),
-    ("ocx", 1, 0), ("o", 2, 2), ("o", 6, 0), ("q1", 1, 0), ("ocy", 3, 2), ("q2", 2, 0),
-    ("q2", 0, 0), ("ocx", 2, 0), ("ocx", 2, 2), ("ocx", 1, 2), ("ocx", 0, 1), ("ocx", 3, 2),
-    ("ocy", 1, 2), ("o", 6, 2), ("att", 0, 0), ("o", 6, 1), ("q2", 1, 0), ("ocx", 0, 0),
-    ("ocy", 2, 2), ("o", 7, 2), ("att", 1, 0), ("att", 2, 0), ("share", 0, 0), ("o", 7, 1),
-    ("fin", 5, 0), ("fin", 4, 0), ("fin", 0, 0), ("fin", 3, 0), ("fin", 6, 0), ("fin", 2, 0),
-    ("fin", 1, 0), ("fin", 7, 0),
+    ("owno", 2, 0), ("owno", 1, 0), ("owno", 0, 0), ("o", 2, 0), ("own", 0, 0), ("own", 2, 0),
+    ("w", 0, 0), ("own", 1, 0), ("o", 1, 0), ("o", 2, 1), ("w", 0, 1), ("w", 1, 0),
+    ("owno", 3, 0), ("ocy", 1, 0), ("o", 0, 0), ("t", 0, 0), ("ocy", 2, 1), ("o", 1, 1),
+    ("o", 0, 2), ("o", 1, 2), ("w", 0, 2), ("ocy", 0, 2), ("o", 0, 1), ("ocy", 1, 2), ("w", 1, 2),
+    ("w", 1, 1), ("ocy", 1, 1), ("ocy", 0, 0), ("w", 2, 0), ("ocy", 0, 1), ("kv1", 0, 0),
+    ("w", 2, 1), ("q1", 0, 0), ("w", 2, 2), ("ocx", 2, 0), ("kv2", 0, 0), ("ocy", 2, 0),
+    ("ocx", 1, 0), ("o", 2, 2), ("ocx", 0, 2), ("ocx", 0, 0), ("ocx", 1, 2), ("ocx", 0, 1),
+    ("q2", 0, 0), ("ocx", 1, 1), ("o", 3, 0), ("q1", 1, 0), ("ocy", 2, 2), ("att", 0, 0),
+    ("o", 3, 2), ("ocx", 2, 2), ("ocx", 2, 1), ("share", 0, 0), ("pre", 1, 0), ("o", 3, 1),
+    ("q2", 1, 0), ("att", 1, 0), ("pre", 0, 0), ("share", 1, 0), ("pre", 2, 0), ("fin", 1, 0),
+    ("fin", 0, 0), ("fin", 2, 0), ("pre", 3, 0), ("fin", 3, 0),
 )
 ORDER_INNER = (
-    ("owno", 3, 0), ("owno", 2, 0), ("own", 0, 0), ("owno", 0, 0), ("o", 3, 0), ("o", 2, 0),
-    ("w", 0, 1), ("owno", 5, 0), ("own", 1, 0), ("w", 0, 0), ("w", 0, 2), ("owno", 4, 0),
-    ("o", 0, 0), ("owno", 1, 0), ("o", 4, 1), ("o", 0, 1), ("o", 5, 1), ("o", 1, 0), ("o", 4, 2),
-    ("o", 5, 0), ("w", 3, 1), ("w", 1, 1), ("o", 4, 0), ("t", 0, 0), ("o", 3, 1), ("o", 5, 2),
-    ("ocy", 5, 1), ("kv1", 0, 0), ("w", 1, 0), ("ocy", 0, 0), ("ocx", 1, 0), ("w", 1, 2),
-    ("ocy", 1, 0), ("own", 2, 0), ("o", 0, 2), ("own", 3, 0), ("ocy", 4, 0), ("w", 3, 2),
-    ("ocy", 2, 0), ("w", 2, 1), ("w", 3, 0), ("o", 3, 2), ("w", 2, 0), ("ocx", 0, 2), ("o", 1, 1),
-    ("ocy", 5, 2), ("w", 2, 2), ("ocy", 3, 1), ("o", 1, 2), ("ocy", 4, 2), ("ocx", 4, 0),
-    ("owno", 6, 0), ("ocy", 3, 0), ("ocy", 0, 1), ("owno", 7, 0), ("ocx", 0, 0), ("o", 6, 1),
-    ("ocx", 0, 1), ("q1", 0, 0), ("ocx", 1, 2), ("o", 2, 1), ("o", 2, 2), ("q1", 2, 0),
-    ("ocx", 4, 1), ("o", 7, 1), ("ocx", 2, 0), ("ocy", 4, 1), ("kv2", 0, 0), ("ocx", 5, 1),
-    ("o", 6, 2), ("q2", 0, 0), ("ocy", 5, 0), ("ocx", 3, 2), ("o", 6, 0), ("q1", 1, 0),
-    ("ocy", 1, 2), ("o", 7, 2), ("o", 7, 0), ("ocx", 5, 2), ("ocy", 0, 2), ("att", 0, 0),
-    ("q2", 1, 0), ("ocy", 3, 2), ("ocx", 2, 1), ("ocx", 1, 1), ("ocy", 1, 1), ("ocx", 5, 0),
-    ("ocx", 3, 0), ("q2", 2, 0), ("ocx", 4, 2), ("att", 1, 0), ("att", 2, 0), ("ocy", 2, 2),
-    ("ocx", 3, 1), ("ocx", 2, 2), ("share", 0, 0), ("ocy", 2, 1), ("fin", 0, 0), ("fin", 6, 0),
-    ("fin", 1, 0), ("fin", 7, 0), ("fin", 5, 0), ("fin", 3, 0), ("fin", 4, 0), ("fin", 2, 0),
+    ("owno", 2, 0), ("own", 0, 0), ("o", 2, 0), ("owno", 1, 0), ("o", 1, 1), ("w", 0, 0),
+    ("own", 1, 0), ("o", 0, 1), ("w", 0, 1), ("o", 1, 0), ("ocy", 2, 0), ("ocy", 1, 1),
+    ("owno", 0, 0), ("ocy", 0, 1), ("t", 0, 0), ("w", 1, 1), ("o", 1, 2), ("o", 0, 2),
+    ("w", 0, 2), ("o", 0, 0), ("w", 1, 2), ("w", 2, 1), ("w", 1, 0), ("own", 2, 0), ("ocy", 1, 0),
+    ("o", 2, 1), ("w", 2, 0), ("w", 2, 2), ("ocy", 0, 0), ("o", 2, 2), ("o", 3, 1), ("ocx", 2, 0),
+    ("ocx", 1, 2), ("kv1", 0, 0), ("ocy", 1, 2), ("ocx", 0, 0), ("owno", 3, 0), ("ocx", 0, 2),
+    ("ocy", 2, 1), ("ocx", 1, 0), ("ocy", 0, 2), ("q1", 0, 0), ("kv2", 0, 0), ("ocx", 2, 2),
+    ("o", 3, 2), ("ocx", 2, 1), ("q1", 1, 0), ("ocx", 1, 1), ("ocx", 0, 1), ("ocy", 2, 2),
+    ("o", 3, 0), ("q2", 0, 0), ("att", 0, 0), ("share", 0, 0), ("q2", 1, 0), ("att", 1, 0),
+    ("share", 1, 0), ("pre", 2, 0), ("pre", 0, 0), ("pre", 1, 0), ("fin", 2, 0), ("fin", 0, 0),
+    ("pre", 3, 0), ("fin", 3, 0), ("fin", 1, 0),
 )
 
 
@@ -154,6 +141,7 @@
 class Run:
     def __init__(self, ends):
         self.ends = ends
+        self.shared = 0
         self.sent = collections.defaultdict(int)
 
     def begin(self, c, kind, ref):
@@ -164,7 +152,7 @@
 def kernel(
     n, tokens, query_w, key_w, value_w, out_w, listing, live_in, mixed,
     tok, other, weights, outs, lists, table, picked, mine_kv, mine_q, away, back,
-    queries, bias, attended, chosen, live, local_sem, send_sem, recv_sem,
+    queries, bias, attended, summed, chosen, live, local_sem, send_sem, recv_sem,
 ):
     dp, me, tp = lax.axis_index("dp"), lax.axis_index("kv"), lax.axis_index("tp")
     x_at, y_at = lax.rem(dp, 2), lax.div(dp, 2)
@@ -206,9 +194,14 @@
         remote(ref, ref, 0, recv, partner).wait_recv()
 
     barrier = pltpu.get_barrier_semaphore()
-    greeted = [{"kv": lax.rem(me + step, n)} for step in range(1, n)] + [to_x, to_y, partner]
-    for target in greeted:
+
+    def greet(target):
         pl.semaphore_signal(barrier, inc=1, device_id=target, device_id_type=MESH)
+
+    pl.when(me < n - 1)(lambda: greet({"kv": right}))
+    pl.when(me > 0)(lambda: greet({"kv": left}))
+    for target in (to_x, to_y, partner):
+        greet(target)
 
     my_rows = pl.ds(pl.multiple_of(x_at * seg, seg), seg)
     my_slab = pl.ds(pl.multiple_of(me * seg, seg), seg)
@@ -235,7 +228,7 @@
         )
 
     with jax.named_scope("barrier"):
-        pl.semaphore_wait(barrier, len(greeted))
+        pl.semaphore_wait(barrier, jnp.where(is_end, 4, 5))
 
     others = n - 1
     W = 0
@@ -274,8 +267,7 @@
             listing, lists.at[me], LISTS + step - 1, L + step - 1, {"kv": jnp.maximum(me - step, 0)}
         )
 
-    for step in range(1, n):
-        pl.when(me >= step)(l_copy(step).start)
+    pl.when(me >= 1)(l_copy(1).start)
 
     def z_targets(run):
         return [inward] if run.ends else [{"kv": right}, {"kv": left}]
@@ -468,22 +460,39 @@
             )
             attended[tp, :, cols] = jnp.where(alive, summed / total, 0.0).astype(jnp.bfloat16)
 
-    def share(run):
-        piece = attended.at[tp]
-        run.begin(remote(piece, piece, REST, S, partner), REST, piece)
-        arrived(attended.at[1 - tp], S)
+    def of_group(which, group):
+        return attended.at[which, :, firsts[group] : firsts[group] + widths[group]]
+
+    def share(run, group):
+        piece = of_group(tp, group)
+        run.begin(remote(piece, piece, REST, S + group - 1, partner), REST, piece)
+
+    def shared(run, last):
+        while run.shared < last:
+            run.shared += 1
+            arrived(of_group(1 - tp, run.shared), S + run.shared - 1)
 
     wide = queries.shape[1]
 
-    def final(s):
+    def mix(s, first, last):
+        acc = jnp.zeros((rows, tiles[s]), jnp.float32)
+        for which in range(2):
+            acc += jnp.dot(
+                attended[which, :, first:last],
+                outs[s][which * wide + first : which * wide + last, :],
+                preferred_element_type=jnp.float32,
+            )
+        return acc
+
+    def early(run, s):
+        shared(run, 1)
         o_arrive(s)
-        acc = jnp.dot(
-            attended[0], outs[s][:wide, :], preferred_element_type=jnp.float32
-        )
-        acc += jnp.dot(
-            attended[1], outs[s][wide:, :], preferred_element_type=jnp.float32
-        )
-        mixed[:, sum(tiles[:s]) : sum(tiles[: s + 1])] = acc.astype(jnp.bfloat16)
+        summed[:, sum(tiles[:s]) : sum(tiles[: s + 1])] = mix(s, 0, widths[1])
+
+    def final(run, s):
+        shared(run, groups - 1)
+        cols = slice(sum(tiles[:s]), sum(tiles[: s + 1]))
+        mixed[:, cols] = (summed[:, cols] + mix(s, widths[1], wide)).astype(jnp.bfloat16)
 
     def settle():
         for owner in range(n):
@@ -511,6 +520,8 @@
         elif name == "ocx" or name == "ocy":
             o_turn(run, i, j, name == "ocx")
         elif name == "kv1":
+            for step in range(2, n):
+                pl.when(me >= step)(l_copy(step).start)
             project(run, 0)
         elif name == "kv2":
             share_blocks(run)
@@ -521,9 +532,11 @@
         elif name == "att":
             attend(1 + i)
         elif name == "share":
-            share(run)
+            share(run, 1 + i)
+        elif name == "pre":
+            early(run, i)
         else:
-            final(i)
+            final(run, i)
 
     def follow(order, ends):
         run = Run(ends)
@@ -573,7 +586,7 @@
     f32 = jnp.float32
     anywhere = pl.BlockSpec(memory_space=pl.ANY)
     others = n - 1
-    arrivals = groups * (others + 2) + chunks * (3 * others + 1) + 2 + 2 * others + 1
+    arrivals = groups * (others + 2) + chunks * (3 * others + 1) + 2 + 2 * others + groups - 1
     return pl.pallas_call(
         functools.partial(kernel, n),
         out_shape=pltpu.VMEM((rows, out_weight.shape[1]), bf16),
@@ -594,6 +607,7 @@
             pltpu.VMEM((rows, wide), bf16),
             pltpu.VMEM((rows, total), f32),
             pltpu.VMEM((2, rows, wide), bf16),
+            pltpu.VMEM((rows, out_weight.shape[1]), f32),
             pltpu.SMEM(chosen.shape, jnp.int32),
             pltpu.SMEM(live_length.shape, jnp.int32),
             dma((groups + chunks + 4,)),

time: 63.3 us -> 60.7 us (0.959)
  Pallas kernels: 61.5 us -> 59 us
    pallas_call x1, Pallas kernels: 61.5 us -> 59 us  [woven_body(): pl.pallas_call(functools.partial(kernel, n), out_shape=pltpu.VMEM((rows,...]
where the time goes in v4:
time: 60.7 us; the launch traced here: 60.6 us
  Pallas kernels  59 us (97%)
  local copies, waits for them, and re-layouts  0.97 us (2%)
  between operations  0.66 us (1%)
    pallas_call x1, Pallas kernels, woven_body(): pl.pallas_call(functools.partial(kernel, n), out_shape=pltpu.VMEM((rows,...  59 us

profile of v4, /device:TPU:0, one launch (start us, length us, event | category | flops | bytes accessed | tf_op | source)
XLA Modules:
  0.0 60.6 jit_solution(14955507860305644287)
XLA Ops:
  0.7 59.0 %shard_map.73 = bf16[256,2048]{1,0:T(8,128)(2,1)S(1)} custom-call(bf16[256,4096]{1,0:T(8,128)(2,1)} %tokens.1, bf16[1024,512]{1,0:T(8,128)(2,1)} %query_w.1, bf16[1024,128]{1,0:T(8,128)(2,1)} %key_w.1, bf16[1024,128]{1,0:T(8,128)(2,1)} %value_w.1, bf16[256,2048]{1,0:T(8,128)(2,1)} %out_w.1, s32[8,16]{1,0:T(8,128)} %listing.1, s32[1]{0:T(128)S(6)} %copy.10.live_in), custom_call_target="tpu_custom_call" | custom-call | tf_op jit(solution)/shard_map/pallas_call | solution.py:590
  59.6 1.0 %copy.9 = bf16[256,2048]{1,0:T(8,128)(2,1)} copy(bf16[256,2048]{1,0:T(8,128)(2,1)S(1)} %shard_map.73) | data formatting | bytes 2097152

commit v5 on v4

--- a/solution.py
+++ b/solution.py
@@ -97,37 +97,40 @@
     return mixed.astype(jnp.bfloat16)
 
 
-HALF = 2
 LEAST = 16
-CUTS = {"q": 32, "p": 16}
-MODES = "ppph"
-SHARES = (4, 4, 4, 4)
-HEADS = (2, 2)
+CUTS = {"q": 32, "p": 16, "s": 0}
+MODES = "qqqh"
+SHARES = (5, 4, 4, 3)
+HEADS = (2, 1, 1)
 ORDER_END = (
-    ("owno", 2, 0), ("owno", 1, 0), ("owno", 0, 0), ("o", 2, 0), ("own", 0, 0), ("own", 2, 0),
-    ("w", 0, 0), ("own", 1, 0), ("o", 1, 0), ("o", 2, 1), ("w", 0, 1), ("w", 1, 0),
-    ("owno", 3, 0), ("ocy", 1, 0), ("o", 0, 0), ("t", 0, 0), ("ocy", 2, 1), ("o", 1, 1),
-    ("o", 0, 2), ("o", 1, 2), ("w", 0, 2), ("ocy", 0, 2), ("o", 0, 1), ("ocy", 1, 2), ("w", 1, 2),
-    ("w", 1, 1), ("ocy", 1, 1), ("ocy", 0, 0), ("w", 2, 0), ("ocy", 0, 1), ("kv1", 0, 0),
-    ("w", 2, 1), ("q1", 0, 0), ("w", 2, 2), ("ocx", 2, 0), ("kv2", 0, 0), ("ocy", 2, 0),
-    ("ocx", 1, 0), ("o", 2, 2), ("ocx", 0, 2), ("ocx", 0, 0), ("ocx", 1, 2), ("ocx", 0, 1),
-    ("q2", 0, 0), ("ocx", 1, 1), ("o", 3, 0), ("q1", 1, 0), ("ocy", 2, 2), ("att", 0, 0),
-    ("o", 3, 2), ("ocx", 2, 2), ("ocx", 2, 1), ("share", 0, 0), ("pre", 1, 0), ("o", 3, 1),
-    ("q2", 1, 0), ("att", 1, 0), ("pre", 0, 0), ("share", 1, 0), ("pre", 2, 0), ("fin", 1, 0),
-    ("fin", 0, 0), ("fin", 2, 0), ("pre", 3, 0), ("fin", 3, 0),
+    ("owno", 0, 0), ("owno", 1, 0), ("o", 2, 0), ("own", 0, 0), ("owno", 2, 0), ("o", 1, 0),
+    ("own", 2, 0), ("o", 2, 1), ("ocy", 2, 0), ("own", 1, 0), ("own", 3, 0), ("tf", 0, 0),
+    ("ocy", 2, 1), ("ocx", 2, 0), ("o", 1, 1), ("o", 0, 2), ("ocx", 2, 1), ("ocy", 1, 0),
+    ("w", 0, 0), ("owno", 3, 0), ("w", 0, 1), ("t", 0, 0), ("o", 1, 2), ("o", 0, 1),
+    ("ocy", 0, 2), ("o", 0, 0), ("ocy", 1, 2), ("w", 0, 2), ("ocx", 1, 0), ("o", 2, 2),
+    ("kv1", 0, 0), ("ocy", 1, 1), ("ocy", 0, 0), ("ocx", 0, 1), ("ocx", 0, 2), ("w", 2, 0),
+    ("w", 1, 2), ("ocx", 1, 2), ("ocx", 1, 1), ("mid", 0, 0), ("ocx", 2, 2), ("w", 1, 1),
+    ("w", 1, 0), ("ocy", 2, 2), ("q1", 0, 0), ("kv2", 0, 0), ("w", 2, 2), ("w", 2, 1),
+    ("ocx", 0, 0), ("ocy", 0, 1), ("q1", 1, 0), ("w", 3, 2), ("mid", 1, 0), ("w", 3, 0),
+    ("w", 3, 1), ("q1", 2, 0), ("mid", 2, 0), ("q2", 0, 0), ("o", 3, 0), ("att", 0, 0),
+    ("mid", 3, 0), ("share", 0, 0), ("o", 3, 2), ("q2", 1, 0), ("att", 1, 0), ("share", 1, 0),
+    ("pre", 1, 0), ("o", 3, 1), ("q2", 2, 0), ("att", 2, 0), ("share", 2, 0), ("pre", 2, 0),
+    ("pre", 0, 0), ("fin", 2, 0), ("fin", 1, 0), ("pre", 3, 0), ("fin", 0, 0), ("fin", 3, 0),
 )
 ORDER_INNER = (
-    ("owno", 2, 0), ("own", 0, 0), ("o", 2, 0), ("owno", 1, 0), ("o", 1, 1), ("w", 0, 0),
-    ("own", 1, 0), ("o", 0, 1), ("w", 0, 1), ("o", 1, 0), ("ocy", 2, 0), ("ocy", 1, 1),
-    ("owno", 0, 0), ("ocy", 0, 1), ("t", 0, 0), ("w", 1, 1), ("o", 1, 2), ("o", 0, 2),
-    ("w", 0, 2), ("o", 0, 0), ("w", 1, 2), ("w", 2, 1), ("w", 1, 0), ("own", 2, 0), ("ocy", 1, 0),
-    ("o", 2, 1), ("w", 2, 0), ("w", 2, 2), ("ocy", 0, 0), ("o", 2, 2), ("o", 3, 1), ("ocx", 2, 0),
-    ("ocx", 1, 2), ("kv1", 0, 0), ("ocy", 1, 2), ("ocx", 0, 0), ("owno", 3, 0), ("ocx", 0, 2),
-    ("ocy", 2, 1), ("ocx", 1, 0), ("ocy", 0, 2), ("q1", 0, 0), ("kv2", 0, 0), ("ocx", 2, 2),
-    ("o", 3, 2), ("ocx", 2, 1), ("q1", 1, 0), ("ocx", 1, 1), ("ocx", 0, 1), ("ocy", 2, 2),
-    ("o", 3, 0), ("q2", 0, 0), ("att", 0, 0), ("share", 0, 0), ("q2", 1, 0), ("att", 1, 0),
-    ("share", 1, 0), ("pre", 2, 0), ("pre", 0, 0), ("pre", 1, 0), ("fin", 2, 0), ("fin", 0, 0),
-    ("pre", 3, 0), ("fin", 3, 0), ("fin", 1, 0),
+    ("owno", 2, 0), ("owno", 1, 0), ("own", 0, 0), ("o", 1, 1), ("o", 2, 0), ("o", 0, 1),
+    ("owno", 0, 0), ("o", 1, 0), ("w", 0, 0), ("w", 0, 1), ("o", 2, 1), ("tf", 0, 0), ("o", 0, 2),
+    ("o", 0, 0), ("o", 1, 2), ("w", 1, 1), ("w", 0, 2), ("own", 2, 0), ("o", 2, 2), ("w", 2, 1),
+    ("t", 0, 0), ("ocy", 0, 1), ("own", 1, 0), ("ocy", 1, 1), ("o", 3, 1), ("ocx", 0, 0),
+    ("w", 1, 2), ("kv1", 0, 0), ("w", 1, 0), ("ocx", 0, 1), ("w", 2, 0), ("ocx", 0, 2),
+    ("w", 2, 2), ("ocx", 1, 1), ("own", 3, 0), ("ocy", 1, 2), ("q1", 1, 0), ("w", 3, 1),
+    ("q1", 0, 0), ("w", 3, 2), ("w", 3, 0), ("ocy", 0, 2), ("ocy", 2, 2), ("mid", 0, 0),
+    ("owno", 3, 0), ("ocx", 1, 2), ("q1", 2, 0), ("mid", 1, 0), ("kv2", 0, 0), ("mid", 2, 0),
+    ("mid", 3, 0), ("ocx", 2, 1), ("o", 3, 2), ("o", 3, 0), ("q2", 1, 0), ("q2", 0, 0),
+    ("ocy", 2, 0), ("q2", 2, 0), ("ocx", 1, 0), ("ocy", 0, 0), ("att", 0, 0), ("ocy", 1, 0),
+    ("ocx", 2, 2), ("ocy", 2, 1), ("share", 0, 0), ("att", 1, 0), ("ocx", 2, 0), ("att", 2, 0),
+    ("pre", 3, 0), ("share", 2, 0), ("share", 1, 0), ("pre", 0, 0), ("pre", 1, 0), ("fin", 1, 0),
+    ("pre", 2, 0), ("fin", 0, 0), ("fin", 2, 0), ("fin", 3, 0),
 )
 
 
@@ -142,6 +145,7 @@
     def __init__(self, ends):
         self.ends = ends
         self.shared = 0
+        self.projected = False
         self.sent = collections.defaultdict(int)
 
     def begin(self, c, kind, ref):
@@ -151,7 +155,7 @@
 
 def kernel(
     n, tokens, query_w, key_w, value_w, out_w, listing, live_in, mixed,
-    tok, other, weights, outs, lists, table, picked, mine_kv, mine_q, away, back,
+    tok, other, crossing, held, weights, outs, lists, table, picked, mine, passing, away, back, away_on, back_on,
     queries, bias, attended, summed, chosen, live, local_sem, send_sem, recv_sem,
 ):
     dp, me, tp = lax.axis_index("dp"), lax.axis_index("kv"), lax.axis_index("tp")
@@ -163,14 +167,16 @@
     dp_far = 2 * (1 - y_at) + (1 - x_at)
     side = lax.rem(x_at + y_at, 2)
     partner = {"tp": 1 - tp}
-    rows = other.shape[0]
-    depth = tok.shape[1]
+    to_far = {"dp": 2 * (1 - y_at) + (1 - x_at)}
+    rows = tok.shape[0]
+    depth = weights[0].shape[0]
     per_dev = rows // BLOCK
     seg = depth // n
-    half_seg = seg // 2
+    parts = 4
     groups, chunks = len(weights), len(outs)
     widths = [ref.shape[1] for ref in weights]
     firsts = [sum(widths[1:g]) for g in range(groups)]
+    starts = [sum(widths[:g]) for g in range(groups)]
     tiles = [ref.shape[1] for ref in outs]
     owned = outs[0].shape[0] // n
     is_end = jnp.logical_or(me == 0, me == n - 1)
@@ -203,47 +209,47 @@
     for target in (to_x, to_y, partner):
         greet(target)
 
-    my_rows = pl.ds(pl.multiple_of(x_at * seg, seg), seg)
-    my_slab = pl.ds(pl.multiple_of(me * seg, seg), seg)
     for s in range(chunks):
         load(
             out_w.at[:, sum(tiles[:s]) : sum(tiles[: s + 1])],
             outs[s].at[pl.ds(pl.multiple_of(me * owned, owned), owned), :],
             groups + s,
         )
-    load(key_w.at[my_rows, :], weights[0].at[my_slab, :HD], 0)
-    load(value_w.at[my_rows, :], weights[0].at[my_slab, HD:], 0)
+    load(key_w, held[0].at[:, :HD], 0)
+    load(value_w, held[0].at[:, HD:], 0)
     for g in range(1, groups):
-        load(
-            query_w.at[my_rows, firsts[g] : firsts[g] + widths[g]], weights[g].at[my_slab, :], g
-        )
+        load(query_w.at[:, firsts[g] : firsts[g] + widths[g]], held[g], g)
     load(listing, lists.at[me], groups + chunks)
     load(listing, chosen, groups + chunks + 1)
     load(live_in, live, groups + chunks + 2)
-    for k in range(n):
+    def token_cols(owner, index, count):
+        return pl.ds(pl.multiple_of((parts * owner + index) * seg, seg), count * seg)
+
+    for i, owner in enumerate(near):
         load(
-            tokens.at[:, pl.ds(pl.multiple_of((2 * k + x_at) * seg, seg), seg)],
-            tok.at[:, k * seg : (k + 1) * seg],
+            tokens.at[:, token_cols(owner, dp, 1)], tok.at[:, i * seg : (i + 1) * seg],
             groups + chunks + 3,
         )
+    load(
+        tokens.at[:, token_cols(me, 0, parts)], tok.at[:, (n - 1) * seg :], groups + chunks + 3
+    )
 
     with jax.named_scope("barrier"):
         pl.semaphore_wait(barrier, jnp.where(is_end, 4, 5))
 
     others = n - 1
     W = 0
-    WY = W + groups * others
-    O = WY + groups
+    O = W + groups * others
     OX = O + chunks * others
     OY = OX + chunks * others
     OC = OY + chunks * others
     T = OC + chunks
-    L = T + 2
+    L = T + 4
     K = L + others
     Y = K + others
-    S = Y + groups
+    S = Y + 2 * groups
     REST = groups + chunks
-    FORTH, TOKENS, LISTS = REST + 1, REST + 2, REST + 3
+    LATE, CROSS, FORTH, TOKENS, LISTS = (REST + 1 + i for i in range(5))
     BLOCKS = LISTS + others
 
     def from_owner(owner, receiver):
@@ -251,14 +257,31 @@
 
     my_part = pl.ds(pl.multiple_of(tp * (rows // 2), rows // 2), rows // 2)
     their_part = pl.ds(pl.multiple_of((1 - tp) * (rows // 2), rows // 2), rows // 2)
-    for k in range(n):
-        cols = pl.ds(pl.multiple_of((2 * k + 1 - x_at) * seg, seg), seg)
-        remote(
-            tokens.at[my_part, cols], other.at[my_part, k * seg : (k + 1) * seg], TOKENS, T, to_x
-        ).start()
+    few = rows // 4
+    first_rows = [pl.ds(pl.multiple_of(tp * (rows // 2) + i * few, few), few) for i in range(2)]
+
+    def t_send(part, target, to, recv, via):
+        for i, owner in enumerate(near):
+            remote(
+                tokens.at[part, token_cols(owner, target["dp"], 1)],
+                to.at[:, i * seg : (i + 1) * seg], TOKENS, recv, via,
+            ).start()
+
+    t_send(my_part, to_x, other.at[0, my_part], T, to_x)
+    t_send(my_part, to_y, other.at[1, my_part], T, to_y)
+    t_send(first_rows[0], to_far, crossing.at[0], T + 2, to_x)
+    t_send(first_rows[1], to_far, crossing.at[1], T + 3, to_y)
+
+    def t_cross(run):
+        for i, target in enumerate((to_y, to_x)):
+            piece = crossing.at[i]
+            arrived(piece, T + 2 + i)
+            run.begin(
+                remote(piece, other.at[2, first_rows[i]], CROSS, T, target), CROSS, piece
+            )
 
     def t_share(run):
-        piece = other.at[my_part, :]
+        piece = other.at[:, my_part, :]
         arrived(piece, T)
         run.begin(remote(piece, piece, FORTH, T + 1, partner), FORTH, piece)
 
@@ -272,29 +295,25 @@
     def z_targets(run):
         return [inward] if run.ends else [{"kv": right}, {"kv": left}]
 
-    def w_piece(group, owner, which):
-        start = owner * seg + which * half_seg
-        return weights[group].at[pl.ds(pl.multiple_of(start, half_seg), half_seg), :]
+    def w_piece(group, owner):
+        return weights[group].at[pl.ds(pl.multiple_of(owner * seg, seg), seg), :]
 
     def w_own(run, group):
-        loaded(weights[group].at[:seg, :], group)
-        piece = w_piece(group, me, y_at)
+        loaded(held[group], group)
+        source = held[group].at[pl.ds(pl.multiple_of(dp * seg, seg), seg), :]
+        piece = w_piece(group, me)
         for target in z_targets(run):
             recv = W + group * others + from_owner(me, target["kv"])
-            run.begin(remote(piece, piece, group, recv, target), group, piece)
+            run.begin(remote(source, piece, group, recv, target), group, source)
 
     def w_step(run, group, slot):
         owner = near[slot]
-        piece = w_piece(group, owner, y_at)
+        piece = w_piece(group, owner)
         arrived(piece, W + group * others + from_owner(owner, me))
         if not run.ends:
             to = jnp.where(owner < me, right, left)
             recv = W + group * others + from_owner(owner, to)
             run.begin(remote(piece, piece, group, recv, {"kv": to}), group, piece)
-        run.begin(remote(piece, piece, group, WY + group, to_y), group, piece)
-
-    def w_arrive(group):
-        arrived(weights[group].at[: others * half_seg, :], WY + group)
 
     quarter = owned // 4
 
@@ -335,7 +354,8 @@
         at = s * others + from_owner(owner, me)
         if along_x:
             arrived(o_piece(s, owner, dp_x * quarter, quarter), OX + at)
-            o_send(run, s, o_piece(s, owner, dp_x * quarter, cut), OC + s, to_y)
+            if cut:
+                o_send(run, s, o_piece(s, owner, dp_x * quarter, cut), OC + s, to_y)
         else:
             arrived(o_piece(s, owner, dp_y * quarter, quarter), OY + at)
             o_send(run, s, o_piece(s, owner, dp_y * quarter + cut, quarter - cut), OC + s, to_x)
@@ -345,21 +365,69 @@
         arrived(outs[s].at[: others * count * quarter, :], OC + s)
 
     def part(source, group):
-        return jnp.dot(
-            source[...], weights[group][...], preferred_element_type=jnp.float32
+        out = jnp.zeros((rows, widths[group]), jnp.float32)
+        for i, owner in enumerate(near):
+            slab = pl.ds(pl.multiple_of(owner * seg, seg), seg)
+            out += jnp.dot(
+                source[:, i * seg : (i + 1) * seg], weights[group][slab, :],
+                preferred_element_type=jnp.float32,
+            )
+        return out
+
+    def columns(group):
+        return slice(starts[group], starts[group] + widths[group])
+
+    def y_copy(group, along_y):
+        return remote(
+            away[along_y].at[:, columns(group)], back[along_y].at[:, columns(group)], REST,
+            Y + 2 * group, to_y if along_y else to_x,
         )
 
-    def y_copy(group):
-        return remote(away[group], back[group], REST, Y + group, to_x)
+    def on_copy(group, along_y):
+        return remote(
+            away_on[along_y].at[:, columns(group)], back_on[along_y].at[:, columns(group)], LATE,
+            Y + 2 * group + 1, to_y if along_y else to_x,
+        )
 
     def project(run, group):
-        w_arrive(group)
-        away[group][...] = part(other, group).astype(jnp.bfloat16)
-        run.begin(y_copy(group), REST, away[group])
-        if group == 0:
-            mine_kv[...] = part(tok, group)
-        else:
-            mine_q[:, firsts[group] : firsts[group] + widths[group]] = part(tok, group)
+        if not run.projected:
+            arrived(other.at[:, their_part, :], T + 1)
+            run.projected = True
+        cols, half = columns(group), rows // 2
+        far = part(other.at[2], group).astype(jnp.bfloat16)
+        beside = part(other.at[0], group)
+        above = part(other.at[1], group)
+        away[0][:half, cols] = beside[:half].astype(jnp.bfloat16)
+        away[0][half:, cols] = far[:half]
+        away[1][:half, cols] = above[half:].astype(jnp.bfloat16)
+        away[1][half:, cols] = far[half:]
+        for along_y in range(2):
+            run.begin(y_copy(group, along_y), REST, away[along_y].at[:, cols])
+        passing[1, :, cols] = above[:half]
+        passing[0, :, cols] = beside[half:]
+        mine[:, cols] = part(tok, group) + jnp.dot(
+            tok[:, (n - 1) * seg :], held[group][...], preferred_element_type=jnp.float32
+        )
+
+    def pass_on(run, group):
+        cols, half = columns(group), rows // 2
+        arrived(tok.at[:, : 2 * widths[group]], Y + 2 * group)
+        for along_y in (1, 0):
+            took = back[1 - along_y][half:, cols].astype(jnp.float32)
+            away_on[along_y][:, cols] = (passing[along_y, :, cols] + took).astype(jnp.bfloat16)
+            run.begin(on_copy(group, along_y), LATE, away_on[along_y].at[:, cols])
+
+    def collected(group):
+        cols, half = columns(group), rows // 2
+        arrived(tok.at[:, : widths[group]], Y + 2 * group + 1)
+        halves = []
+        for i, along_y in enumerate((1, 0)):
+            halves.append(
+                mine[i * half : (i + 1) * half, cols]
+                + back[1 - along_y][:half, cols].astype(jnp.float32)
+                + back_on[along_y][:, cols].astype(jnp.float32)
+            )
+        return jnp.concatenate(halves, axis=0).astype(jnp.bfloat16)
 
     slots = CAP * BLOCK
     local_at = n * slots
@@ -388,8 +456,7 @@
             pl.when(me >= step)(k_copy(step).wait_recv)
 
     def share_blocks(run):
-        y_copy(0).wait_recv()
-        full = (mine_kv[...] + back[0][...].astype(jnp.float32)).astype(jnp.bfloat16)
+        full = collected(0)
         table[local_at : local_at + rows, :] = full
         full = full.astype(jnp.float32)
         for step in range(1, n):
@@ -435,11 +502,7 @@
             bias[j * BLOCK : (j + 1) * BLOCK, :] = jnp.where(causal, spread, -jnp.inf)
 
     def queries_done(group):
-        y_copy(group).wait_recv()
-        cols = slice(firsts[group], firsts[group] + widths[group])
-        queries[:, cols] = (
-            mine_q[:, cols] + back[group][...].astype(jnp.float32)
-        ).astype(jnp.bfloat16)
+        queries[:, firsts[group] : firsts[group] + widths[group]] = collected(group)
 
     def attend(group):
         if group == 1:
@@ -465,7 +528,7 @@
 
     def share(run, group):
         piece = of_group(tp, group)
-        run.begin(remote(piece, piece, REST, S + group - 1, partner), REST, piece)
+        run.begin(remote(piece, piece, LATE, S + group - 1, partner), LATE, piece)
 
     def shared(run, last):
         while run.shared < last:
@@ -513,6 +576,8 @@
             o_own(run, i)
         elif name == "t":
             t_share(run)
+        elif name == "tf":
+            t_cross(run)
         elif name == "w":
             w_step(run, i, j)
         elif name == "o":
@@ -523,6 +588,8 @@
             for step in range(2, n):
                 pl.when(me >= step)(l_copy(step).start)
             project(run, 0)
+        elif name == "mid":
+            pass_on(run, i)
         elif name == "kv2":
             share_blocks(run)
         elif name == "q1":
@@ -541,28 +608,26 @@
     def follow(order, ends):
         run = Run(ends)
         begun = False
-        projected = False
         for name, i, j in order:
             if not begun and not name.startswith("own"):
                 settle()
                 begun = True
-            if not projected and name in ("kv1", "q1"):
-                arrived(other.at[their_part, :], T + 1)
-                projected = True
             with jax.named_scope(f"{name}_{i}_{j}"):
                 act(run, name, i, j)
         for kind, size in run.sent.items():
-            if kind < groups:
-                ref = weights[kind].at[: size // widths[kind], :]
-            elif kind < groups + chunks:
+            if groups <= kind < groups + chunks:
                 ref = outs[kind - groups].at[: size // tiles[kind - groups], :]
+            elif kind < groups or kind in (REST, LATE):
+                ref = tok.at[:, : size // rows]
+            elif kind == CROSS:
+                ref = crossing
             else:
-                ref = tok.at[:, : size // rows]
+                ref = other.at[:, my_part, :]
             remote(ref, ref, kind, 0, partner).wait_send()
 
     pl.when(is_end)(functools.partial(follow, ORDER_END, True))
     pl.when(jnp.logical_not(is_end))(functools.partial(follow, ORDER_INNER, False))
-    ref = other.at[my_part, :]
+    ref = other.at[:, my_part, :]
     remote(ref, ref, TOKENS, T, to_x).wait_send()
     for step in range(1, n):
         pl.when(me >= step)(l_copy(step).wait_send)
@@ -573,12 +638,13 @@
     n = lax.axis_size("kv")
     rows, model = tokens.shape
     wide = query_weight.shape[1]
-    depth = model // HALF
+    seg = model // n // 4
     width = 2 * HD
     widths = [width] + [heads * HD for heads in HEADS]
     unit = out_weight.shape[1] // sum(SHARES)
     tiles = [share * unit for share in SHARES]
     groups, chunks = len(widths), len(tiles)
+    every = sum(widths)
     slots = CAP * BLOCK
     total = n * slots + rows
     dma = pltpu.SemaphoreType.DMA
@@ -586,24 +652,28 @@
     f32 = jnp.float32
     anywhere = pl.BlockSpec(memory_space=pl.ANY)
     others = n - 1
-    arrivals = groups * (others + 2) + chunks * (3 * others + 1) + 2 + 2 * others + groups - 1
+    arrivals = groups * (others + 2) + chunks * (3 * others + 1) + 4 + 2 * others + groups - 1
     return pl.pallas_call(
         functools.partial(kernel, n),
         out_shape=pltpu.VMEM((rows, out_weight.shape[1]), bf16),
         in_specs=[anywhere] * 7,
         out_specs=pl.BlockSpec(memory_space=pltpu.VMEM),
         scratch_shapes=[
-            pltpu.VMEM((rows, depth), bf16),
-            pltpu.VMEM((rows, depth), bf16),
-            tuple(pltpu.VMEM((depth, w), bf16) for w in widths),
+            pltpu.VMEM((rows, (n - 1) * seg + model // n), bf16),
+            pltpu.VMEM((3, rows, (n - 1) * seg), bf16),
+            pltpu.VMEM((2, rows // 4, (n - 1) * seg), bf16),
+            tuple(pltpu.VMEM((key_weight.shape[0], w), bf16) for w in widths),
+            tuple(pltpu.VMEM((n * seg, w), bf16) for w in widths),
             tuple(pltpu.VMEM((n * out_weight.shape[0], w), bf16) for w in tiles),
             pltpu.VMEM((n,) + chosen.shape, jnp.int32),
             pltpu.VMEM((total, width), bf16),
             pltpu.VMEM((n - 1, slots, width), bf16),
-            pltpu.VMEM((rows, width), f32),
-            pltpu.VMEM((rows, wide), f32),
-            tuple(pltpu.VMEM((rows, w), bf16) for w in widths),
-            tuple(pltpu.VMEM((rows, w), bf16) for w in widths),
+            pltpu.VMEM((rows, every), f32),
+            pltpu.VMEM((2, rows // 2, every), f32),
+            tuple(pltpu.VMEM((rows, every), bf16) for _ in range(2)),
+            tuple(pltpu.VMEM((rows, every), bf16) for _ in range(2)),
+            tuple(pltpu.VMEM((rows // 2, every), bf16) for _ in range(2)),
+            tuple(pltpu.VMEM((rows // 2, every), bf16) for _ in range(2)),
             pltpu.VMEM((rows, wide), bf16),
             pltpu.VMEM((rows, total), f32),
             pltpu.VMEM((2, rows, wide), bf16),
@@ -611,7 +681,7 @@
             pltpu.SMEM(chosen.shape, jnp.int32),
             pltpu.SMEM(live_length.shape, jnp.int32),
             dma((groups + chunks + 4,)),
-            dma((groups + chunks + 3 + 2 * others,)),
+            dma((groups + chunks + 5 + 2 * others,)),
             dma((arrivals,)),
         ],
         compiler_params=pltpu.CompilerParams(

time: 60.7 us -> 58.6 us (0.965)
  Pallas kernels: 59 us -> 56.8 us
    pallas_call x1, Pallas kernels: 59 us -> 56.8 us  [woven_body(): pl.pallas_call(functools.partial(kernel, n), out_shape=pltpu.VMEM((rows,...]
where the time goes in v5:
time: 58.6 us; the launch traced here: 58.4 us
  Pallas kernels  56.8 us (97%)
  local copies, waits for them, and re-layouts  0.97 us (2%)
  between operations  0.66 us (1%)
    pallas_call x1, Pallas kernels, woven_body(): pl.pallas_call(functools.partial(kernel, n), out_shape=pltpu.VMEM((rows,...  56.8 us

profile of v5, /device:TPU:0, one launch (start us, length us, event | category | flops | bytes accessed | tf_op | source)
XLA Modules:
  0.0 58.4 jit_solution(470927482652502704)
XLA Ops:
  0.7 56.8 %shard_map.73 = bf16[256,2048]{1,0:T(8,128)(2,1)S(1)} custom-call(bf16[256,4096]{1,0:T(8,128)(2,1)} %tokens.1, bf16[1024,512]{1,0:T(8,128)(2,1)} %query_w.1, bf16[1024,128]{1,0:T(8,128)(2,1)} %key_w.1, bf16[1024,128]{1,0:T(8,128)(2,1)} %value_w.1, bf16[256,2048]{1,0:T(8,128)(2,1)} %out_w.1, s32[8,16]{1,0:T(8,128)} %listing.1, s32[1]{0:T(128)S(6)} %copy.10.live_in), custom_call_target="tpu_custom_call" | custom-call | tf_op jit(solution)/shard_map/pallas_call | solution.py:656
  57.5 1.0 %copy.9 = bf16[256,2048]{1,0:T(8,128)(2,1)} copy(bf16[256,2048]{1,0:T(8,128)(2,1)S(1)} %shard_map.73) | data formatting | bytes 2097152

commit v6 on v5

--- a/solution.py
+++ b/solution.py
@@ -145,6 +145,7 @@
     def __init__(self, ends):
         self.ends = ends
         self.shared = 0
+        self.whole = set()
         self.projected = False
         self.sent = collections.defaultdict(int)
 
@@ -555,7 +556,11 @@
     def final(run, s):
         shared(run, groups - 1)
         cols = slice(sum(tiles[:s]), sum(tiles[: s + 1]))
-        mixed[:, cols] = (summed[:, cols] + mix(s, widths[1], wide)).astype(jnp.bfloat16)
+        if s in run.whole:
+            o_arrive(s)
+            mixed[:, cols] = mix(s, 0, wide).astype(jnp.bfloat16)
+        else:
+            mixed[:, cols] = (summed[:, cols] + mix(s, widths[1], wide)).astype(jnp.bfloat16)
 
     def settle():
         for owner in range(n):
@@ -608,7 +613,10 @@
     def follow(order, ends):
         run = Run(ends)
         begun = False
-        for name, i, j in order:
+        for at, (name, i, j) in enumerate(order):
+            if name == "pre" and order[at + 1] == ("fin", i, j):
+                run.whole.add(i)
+                continue
             if not begun and not name.startswith("own"):
                 settle()
                 begun = True

time: 58.6 us -> 58.6 us (level)
  no operation moved by 1% of the time
where the time goes in v6:
time: 58.6 us; the launch traced here: 58.4 us
  Pallas kernels  56.7 us (97%)
  local copies, waits for them, and re-layouts  0.97 us (2%)
  between operations  0.66 us (1%)
    pallas_call x1, Pallas kernels, woven_body(): pl.pallas_call(functools.partial(kernel, n), out_shape=pltpu.VMEM((rows,...  56.7 us

profile of v6, /device:TPU:0, one launch (start us, length us, event | category | flops | bytes accessed | tf_op | source)
XLA Modules:
  0.0 58.4 jit_solution(18121370556780161793)
XLA Ops:
  0.7 56.7 %shard_map.73 = bf16[256,2048]{1,0:T(8,128)(2,1)S(1)} custom-call(bf16[256,4096]{1,0:T(8,128)(2,1)} %tokens.1, bf16[1024,512]{1,0:T(8,128)(2,1)} %query_w.1, bf16[1024,128]{1,0:T(8,128)(2,1)} %key_w.1, bf16[1024,128]{1,0:T(8,128)(2,1)} %value_w.1, bf16[256,2048]{1,0:T(8,128)(2,1)} %out_w.1, s32[8,16]{1,0:T(8,128)} %listing.1, s32[1]{0:T(128)S(6)} %copy.10.live_in), custom_call_target="tpu_custom_call" | custom-call | tf_op jit(solution)/shard_map/pallas_call | solution.py:664
  57.4 1.0 %copy.9 = bf16[256,2048]{1,0:T(8,128)(2,1)} copy(bf16[256,2048]{1,0:T(8,128)(2,1)S(1)} %shard_map.73) | data formatting | bytes 2097152
